TPU v7x, 32 devices: a whole 2x2x4 slice. The times are simulated.
32 devices in a mesh: sp: 8 (over z, y), tp: 4 (over x, core).
Axes of the slice: x: 2, y: 2, z: 4, core: 2. Of those that a mesh axis runs over, the one named last changes fastest.
Arguments:
- residual: bfloat16 [2048, 2048], P('sp'), may hold values from -6 to 6
- queries: bfloat16 [2048, 8, 2, 128], P('sp', 'tp'), may hold values from -100 to 100
- key_rows: bfloat16 [2048, 8, 2, 128], P('sp', 'tp'), may hold values from -6 to 6
- values: bfloat16 [2048, 8, 256], P('sp', 'tp'), may hold values from -6 to 6
- lambda_head: float32 [8], P('tp'), may hold values from 0.3 to 0.8
- sub_gain: float32 [256], replicated, may hold values from 0.1 to 1.9
- w_out: bfloat16 [2048, 2048], P('tp'), may hold values from -0.125 to 0.125
- norm_gain: float32 [2048], replicated, may hold values from 0.1 to 1.9
- w_gate: bfloat16 [2048, 5632], P('sp', 'tp'), may hold values from -0.125 to 0.125
- w_up: bfloat16 [2048, 5632], P('sp', 'tp'), may hold values from -0.125 to 0.125
- conv_gate: float32 [3, 5632], P(None, 'tp'), may hold values from -3 to 3
- conv_up: float32 [3, 5632], P(None, 'tp'), may hold values from -3 to 3
- w_down: bfloat16 [5632, 2048], P('tp'), may hold values from -0.078125 to 0.078125
Outputs:
- layer_out: bfloat16 [2048, 2048], P(('sp', 'tp'))
All inputs are finite; a program needn't handle non-finite values.
Results may differ from a plain program's by a relative error of at most 0.017.
Values may be sent and summed in bfloat16 or wider, within the bound.
A program may use at most 192 MiB of HBM per device.

v0:
```python
import functools
import math

import jax
import jax.numpy as jnp
from jax import lax
from jax.experimental import pallas as pl
from jax.experimental.pallas import tpu as pltpu
from jax.sharding import PartitionSpec as P

MESH = pl.DeviceIdType.MESH
epsilon = 1e-06
lambda_init = 0.8 - 0.6 * math.exp(-0.3)
bf16 = jnp.bfloat16
f32 = jnp.float32
HALO = 16
UP, DOWN, ACROSS = 0, 1, 2
KV, GATE, UP_A, UP_B = 0, 1, 2, 3


def kernel(
    S, T, heads, dh, dv,
    q_hbm, kv_hbm, res_hbm, wout_hbm, wg_hbm, wu_hbm, wd_hbm,
    lam_ref, sub_ref, norm_ref, cg_ref, cu_ref,
    out_ref,
    q, kv, res, wout, wg, wua, wub, wd,
    m_s, l_s, acc_s, n_own, n_in, part, part_in, mid, hn, hb, halo_in, acc_g, acc_u, hid, low, low_in,
    local_sem, pair_sem, send_sem, recv_sem, tp_send, tp_recv, halo_sem, low_send, low_recv,
):
    Z = S // 2
    sp = lax.axis_index("sp")
    tp = lax.axis_index("tp")
    z = lax.div(sp, 2)
    y = lax.rem(sp, 2)
    rows = q.shape[1]
    feat = wg.shape[1]
    tail = wub.shape[2]
    split = wua.shape[2]
    hh = heads // 2
    kw = 2 * hh * dh
    D = wout.shape[1]
    own = rows // T
    units = wg.shape[2]
    has_up, has_down = z < Z - 1, z > 0
    has_next, has_prev = sp < S - 1, sp > 0

    def one(flag):
        return flag.astype(jnp.int32)

    def peer(d):
        return lax.rem(tp + d, T)

    target = {UP: sp + 2, DOWN: sp - 2, ACROSS: z * 2 + (1 - y)}
    bufs = {KV: kv, GATE: wg, UP_A: wua, UP_B: wub}

    loads = [
        pltpu.make_async_copy(kv_hbm.at[y], kv.at[sp], local_sem.at[0]),
        pltpu.make_async_copy(wg_hbm, wg.at[sp], local_sem.at[1]),
        pltpu.make_async_copy(wu_hbm.at[:, pl.ds(0, split)], wua.at[sp], local_sem.at[2]),
        pltpu.make_async_copy(wu_hbm.at[:, pl.ds(split, tail)], wub.at[sp], local_sem.at[3]),
        pltpu.make_async_copy(q_hbm.at[y], q.at[y], local_sem.at[4]),
        pltpu.make_async_copy(wout_hbm, wout, local_sem.at[5]),
        pltpu.make_async_copy(res_hbm, res, local_sem.at[6]),
        pltpu.make_async_copy(wd_hbm, wd, local_sem.at[7]),
    ]
    for c in loads:
        c.start()

    barrier = pltpu.get_barrier_semaphore()

    def greet(device):
        pl.semaphore_signal(barrier, inc=1, device_id=device, device_id_type=MESH)

    pl.when(has_up)(lambda: greet((target[UP], tp)))
    pl.when(has_down)(lambda: greet((target[DOWN], tp)))
    greet((target[ACROSS], tp))
    pl.when(has_next)(lambda: greet((sp + 1, tp)))
    pl.when(has_prev)(lambda: greet((sp - 1, tp)))
    for d in range(1, T):
        greet((sp, peer(d)))
    pl.semaphore_wait(
        barrier, T + one(has_up) + one(has_down) + one(has_next) + one(has_prev)
    )

    def remote(p, blk, way):
        return pltpu.make_async_remote_copy(
            src_ref=bufs[p].at[blk],
            dst_ref=bufs[p].at[blk],
            send_sem=send_sem.at[way, p, blk],
            recv_sem=recv_sem.at[p, blk],
            device_id=(target[way], tp),
            device_id_type=MESH,
        )

    def send(p, blk, way, cond=None):
        if cond is None:
            remote(p, blk, way).start()
        else:
            pl.when(cond)(lambda: remote(p, blk, way).start())

    def sent(p, blk, way):
        remote(p, blk, way).wait_send()

    def arrive(p, blk):
        remote(p, blk, ACROSS).wait_recv()

    other = 1 - y
    across = (target[ACROSS], tp)

    def pair(src, dst, k):
        return pltpu.make_async_remote_copy(
            src_ref=src, dst_ref=dst, send_sem=pair_sem.at[0, k], recv_sem=pair_sem.at[1, k],
            device_id=across, device_id_type=MESH,
        )

    kv_swap = pair(kv_hbm.at[other], kv.at[sp], 0)
    q_swap = pair(q_hbm.at[other], q.at[y], 1)
    kv_got = pair(kv_hbm.at[other], kv.at[target[ACROSS]], 0)
    q_got = pair(q_hbm.at[other], q.at[other], 1)
    kv_swap.start()
    q_swap.start()
    loads[0].wait()
    send(KV, sp, UP, has_up)
    for p in (UP_B, GATE, UP_A):
        loads[p].wait()
        send(p, sp, DOWN, has_down)
        send(p, sp, ACROSS)
    loads[4].wait()

    m_s[...] = jnp.full(m_s.shape, -1e30, f32)
    l_s[...] = jnp.zeros(l_s.shape, f32)
    acc_s[...] = jnp.zeros(acc_s.shape, f32)
    scale = 1.0 / math.sqrt(dh)

    def attend(yy, blk):
        row_at = (z * 2 + yy) * rows + lax.broadcasted_iota(jnp.int32, (rows, rows), 0)
        col_at = blk * rows + lax.broadcasted_iota(jnp.int32, (rows, rows), 1)
        keep = col_at <= row_at
        for h in range(hh):
            v = kv[blk, :, kw + h * dv : kw + (h + 1) * dv]
            for c in range(2):
                i = 2 * h + c
                k = kv[blk, :, i * dh : (i + 1) * dh]
                s = lax.dot_general(
                    q[yy, :, i * dh : (i + 1) * dh], k, (((1,), (1,)), ((), ())),
                    preferred_element_type=f32,
                ) * scale
                s = jnp.where(keep, s, -1e30)
                old = m_s[yy, i]
                new = jnp.maximum(old, jnp.max(s, axis=1, keepdims=True))
                e = jnp.where(keep, jnp.exp(s - new), 0.0)
                fade = jnp.exp(old - new)
                m_s[yy, i] = new
                l_s[yy, i] = l_s[yy, i] * fade + jnp.sum(e, axis=1, keepdims=True)
                acc_s[yy, i] = acc_s[yy, i] * fade + jnp.dot(
                    e.astype(bf16), v, preferred_element_type=f32
                )

    kv_got.wait_recv()
    q_got.wait_recv()
    send(KV, target[ACROSS], UP, has_up)

    @pl.loop(0, Z)
    def _(r):
        @pl.when(z >= r)
        def _():
            @pl.when(r > 0)
            def _():
                for blk in (sp - 2 * r, target[ACROSS] - 2 * r):
                    arrive(KV, blk)
                    send(KV, blk, UP, has_up)

            @pl.loop(0, 4)
            def _(i):
                yy, c = lax.div(i, 2), lax.rem(i, 2)
                pl.when((r > 0) | (yy >= c))(lambda: attend(yy, (z - r) * 2 + c))

    for p in (UP_B, GATE, UP_A):
        send(p, sp, UP, has_up)

    for yy in range(2):
        for h in range(hh):
            a0 = acc_s[yy, 2 * h] / l_s[yy, 2 * h]
            a1 = acc_s[yy, 2 * h + 1] / l_s[yy, 2 * h + 1]
            a = a0 - lam_ref[y * hh + h] * a1
            ms = jnp.mean(a * a, axis=1, keepdims=True)
            n = a * lax.rsqrt(ms + epsilon) * sub_ref[...] * (1.0 - lambda_init)
            n_own[yy, :, h * dv : (h + 1) * dv] = n.astype(bf16)
    n_swap = pair(n_own.at[other], n_in, 2)
    n_swap.start()

    def relay(r):
        @pl.when((r == 0))
        def _():
            b = z * 2 + (1 - y)
            arrive(UP_B, b)
            send(UP_B, b, UP, has_up)
            send(UP_B, b, DOWN, has_down)

        def side(exists, col_z, way, cond):
            @pl.when(exists & (r > 0))
            def _():
                a = col_z * 2 + y
                b = col_z * 2 + (1 - y)
                for p in (GATE, UP_A, UP_B):
                    arrive(p, a)
                    send(p, a, way, cond)
                    if p != UP_B:
                        send(p, a, ACROSS)
                arrive(UP_B, b)
                send(UP_B, b, way, cond)

        side(z + r < Z, z + r, DOWN, has_down)
        side(z >= r, z - r, UP, has_up)

    first = min(2, Z)

    @pl.loop(0, first)
    def _(r):
        relay(r)

    loads[5].wait()
    n_swap.wait_recv()
    width = min(512, D)
    hw = hh * dv
    for c in range(0, D, width):
        cols = slice(c, c + width)
        part[:, :, cols] = (
            (
                jnp.dot(n_own[y], wout[pl.ds(y * hw, hw), cols], preferred_element_type=f32)
                + jnp.dot(n_in[...], wout[pl.ds(other * hw, hw), cols], preferred_element_type=f32)
            )
            .astype(bf16)
            .reshape(T, own, width)
        )

    def swap(d, src, dst, k):
        return pltpu.make_async_remote_copy(
            src_ref=src, dst_ref=dst, send_sem=tp_send.at[k, d], recv_sem=tp_recv.at[k, d],
            device_id=(sp, peer(d)), device_id_type=MESH,
        )

    firsts = [swap(d, part.at[peer(d)], part_in.at[d], 0) for d in range(1, T)]
    for c in firsts:
        c.start()
    loads[6].wait()
    total = res[pl.ds(tp * own, own), :].astype(f32) + part[tp].astype(f32)
    for d in range(1, T):
        firsts[d - 1].wait_recv()
        total = total + part_in[d].astype(f32)
    mid[...] = total
    ms = jnp.mean(total * total, axis=1, keepdims=True)
    hn[tp] = (total * lax.rsqrt(ms + epsilon) * norm_ref[...]).astype(bf16)
    seconds = [swap(d, hn.at[tp], hn.at[tp], 1) for d in range(1, T)]
    for c in seconds:
        c.start()
    for d in range(1, T):
        back = lax.rem(tp + T - d, T)
        swap(d, hn.at[back], hn.at[back], 1).wait_recv()

    halo = pltpu.make_async_remote_copy(
        src_ref=hn.at[T - 1, pl.ds(own - HALO, HALO)], dst_ref=halo_in,
        send_sem=halo_sem.at[0], recv_sem=halo_sem.at[1],
        device_id=(sp + 1, tp), device_id_type=MESH,
    )
    pl.when(has_next)(halo.start)

    @pl.loop(first, Z)
    def _(r):
        relay(r)

    pl.when(has_prev)(halo.wait_recv)

    @pl.when(jnp.logical_not(has_prev))
    def _():
        halo_in[...] = jnp.zeros(halo_in.shape, bf16)

    for j in range(S):
        hb[j, :HALO, :] = halo_in[:, j * feat : (j + 1) * feat]
        hb[j, HALO:, :] = hn[:, :, j * feat : (j + 1) * feat].reshape(rows, feat)

    acc_g[...] = jnp.zeros(acc_g.shape, f32)
    acc_u[...] = jnp.zeros(acc_u.shape, f32)

    def mul(blk):
        acc_g[...] += jnp.dot(hb[blk], wg[blk], preferred_element_type=f32)
        acc_u[:, :split] += jnp.dot(hb[blk], wua[blk], preferred_element_type=f32)
        acc_u[:, split:] += jnp.dot(hb[blk], wub[blk], preferred_element_type=f32)

    @pl.loop(0, Z)
    def _(k):
        mul(2 * k + y)

    def take(blk):
        arrive(GATE, blk)
        arrive(UP_A, blk)
        mul(blk)

    @pl.loop(0, Z)
    def _(r):
        pl.when((z + r < Z) & (r > 0))(lambda: take((z + r) * 2 + 1 - y))
        pl.when(z >= r)(lambda: take((z - r) * 2 + 1 - y))

    for c in range(0, units, 128):
        cols = slice(c, c + 128)
        g = acc_g[:, cols].astype(bf16).astype(f32)
        u = acc_u[:, cols].astype(bf16).astype(f32)

        def mix(x, taps):
            out = taps[0:1, cols] * x[HALO - 2 : HALO - 2 + rows]
            out = out + taps[1:2, cols] * x[HALO - 1 : HALO - 1 + rows]
            return out + taps[2:3, cols] * x[HALO:]

        gm, um = mix(g, cg_ref), mix(u, cu_ref)
        hid[:, cols] = (gm / (1.0 + jnp.exp(-gm)) * um).astype(bf16)

    loads[7].wait()
    chunks, cw = low.shape[0], low.shape[3]
    lows = []
    for c in range(chunks):
        low[c] = (
            jnp.dot(hid[...], wd[:, c * cw : (c + 1) * cw], preferred_element_type=f32)
            .astype(bf16)
            .reshape(T, own, cw)
        )
        for d in range(1, T):
            copy = pltpu.make_async_remote_copy(
                src_ref=low.at[c, peer(d)], dst_ref=low_in.at[c, d],
                send_sem=low_send.at[c, d], recv_sem=low_recv.at[c, d],
                device_id=(sp, peer(d)), device_id_type=MESH,
            )
            copy.start()
            lows.append(copy)

    @pl.loop(0, Z)
    def _(k):
        a = 2 * k + y
        b = 2 * k + 1 - y
        for p in (GATE, UP_A):
            sent(p, a, ACROSS)
        pl.when(k == z)(lambda: sent(UP_B, a, ACROSS))
        for p, blk in ((KV, a), (KV, b), (GATE, a), (UP_A, a), (UP_B, a), (UP_B, b)):
            pl.when(has_up & (k <= z))(functools.partial(sent, p, blk, UP))
            if p != KV:
                pl.when(has_down & (k >= z))(functools.partial(sent, p, blk, DOWN))

    for c in firsts + seconds + [kv_swap, q_swap, n_swap]:
        c.wait_send()
    pl.when(has_next)(halo.wait_send)

    for c in range(chunks):
        cols = slice(c * cw, (c + 1) * cw)
        total = mid[:, cols] + low[c, tp].astype(f32)
        for d in range(1, T):
            lows[c * (T - 1) + d - 1].wait_recv()
            total = total + low_in[c, d].astype(f32)
        out_ref[:, cols] = total.astype(bf16)
    for c in lows:
        c.wait_send()


def local(
    S, T,
    residual, queries, key_rows, values, lambda_head, sub_gain, w_out, norm_gain,
    w_gate, w_up, conv_gate, conv_up, w_down,
):
    rows, heads, maps, dh = queries.shape
    dv = values.shape[2]
    feat, units = w_gate.shape
    D = w_out.shape[1]
    own = rows // T
    tail = 3 * math.gcd(units, 128)
    hh = heads // 2
    q = queries.reshape(rows, 2, hh * maps * dh).swapaxes(0, 1)
    kv = jnp.concatenate(
        [key_rows.reshape(rows, 2, hh * maps * dh), values.reshape(rows, 2, hh * dv)], axis=2
    ).swapaxes(0, 1)
    kvw = kv.shape[2]
    cw = math.gcd(D, 512)
    chunks = D // cw
    hbm = pl.BlockSpec(memory_space=pl.ANY)
    vmem = pl.BlockSpec(memory_space=pltpu.VMEM)
    smem = pl.BlockSpec(memory_space=pltpu.SMEM)
    padded = rows + HALO
    V = pltpu.VMEM
    dma = pltpu.SemaphoreType.DMA
    return pl.pallas_call(
        functools.partial(kernel, S, T, heads, dh, dv),
        out_shape=jax.ShapeDtypeStruct((own, D), bf16),
        in_specs=[hbm] * 7 + [smem] + [vmem] * 4,
        out_specs=vmem,
        scratch_shapes=[
            V(q.shape, bf16),
            V((S, rows, kvw), bf16),
            V((rows, D), bf16),
            V(w_out.shape, bf16),
            V((S, feat, units), bf16),
            V((S, feat, units - tail), bf16),
            V((S, feat, tail), bf16),
            V(w_down.shape, bf16),
            V((2, 2 * hh, rows, 1), f32),
            V((2, 2 * hh, rows, 1), f32),
            V((2, 2 * hh, rows, dv), f32),
            V((2, rows, hh * dv), bf16),
            V((rows, hh * dv), bf16),
            V((T, own, D), bf16),
            V((T, own, D), bf16),
            V((own, D), f32),
            V((T, own, D), bf16),
            V((S, padded, feat), bf16),
            V((HALO, D), bf16),
            V((padded, units), f32),
            V((padded, units), f32),
            V((rows, units), bf16),
            V((chunks, T, own, cw), bf16),
            V((chunks, T, own, cw), bf16),
            dma((8,)),
            dma((2, 3)),
            dma((3, 4, S)),
            dma((4, S)),
            dma((2, T)),
            dma((2, T)),
            dma((2,)),
            dma((chunks, T)),
            dma((chunks, T)),
        ],
        compiler_params=pltpu.CompilerParams(
            collective_id=0, has_side_effects=True, vmem_limit_bytes=64000000
        ),
    )(
        q, kv, residual, w_out, w_gate, w_up, w_down, lambda_head,
        sub_gain.reshape(1, -1), norm_gain.reshape(1, -1), conv_gate, conv_up,
    )


def solution(mesh):
    placed = (
        P("sp", None),
        P("sp", "tp", None, None),
        P("sp", "tp", None, None),
        P("sp", "tp", None),
        P("tp"),
        P(),
        P("tp", None),
        P(),
        P("sp", "tp"),
        P("sp", "tp"),
        P(None, "tp"),
        P(None, "tp"),
        P("tp", None),
    )
    return jax.shard_map(
        functools.partial(local, mesh.shape["sp"], mesh.shape["tp"]),
        mesh=mesh, in_specs=placed, out_specs=P(("sp", "tp"), None), check_vma=False,
    )
```

profile of v0, /device:TPU:29, one launch (start us, length us, event | category | flops | bytes accessed | tf_op | source)
XLA Modules:
  0.0 174.6 jit_solution(18121421126003016947)
XLA Ops:
  0.0 1.1 reshape.17
  1.2 1.0 copy.16
  2.1 0.8 maximum_bitcast_fusion.kv_hbm
  3.0 1.1 reshape.16
  4.1 0.7 copy.20
  4.8 168.1 %shard_map.127 = bf16[64,2048]{1,0:T(8,128)(2,1)} custom-call(bf16[2,256,256]{2,1,0:T(8,128)(2,1)} %bitcast.7, bf16[2,256,512]{2,1,0:T(8,128)(2,1)} %maximum_bitcast_fusion.kv_hbm, bf16[256,2048]{1,0:T(8,128)(2,1)} %res_hbm.1, bf16[512,2048]{1,0:T(8,128)(2,1)} %wout_hbm.1, bf16[256,1408]{1,0:T(8,128)(2,1)} %wg_hbm.1, bf16[256,1408]{1,0:T(8,128)(2,1)} %wu_hbm.1, ...), custom_call_target="tpu_custom_call" | custom-call | tf_op jit(solution)/shard_map/pallas_call | solution.py:387
  172.9 1.7 copy.22
  (1 shorter events, 0.0 us)
where the time goes:
time: 176 us; the launch traced here: 175 us
  Pallas kernels  168 us (95%)
  local copies, waits for them, and re-layouts  5.65 us (3%)
    pallas_call x1, Pallas kernels, local(): pl.pallas_call(functools.partial(kernel, S, T, heads, dh, dv), out_shape=...  168 us

commit v1 on v0

v1 whole, which is shorter than its diff:
```python
import contextlib
import functools
import math

import jax
import jax.numpy as jnp
from jax import lax
from jax.experimental import pallas as pl
from jax.experimental.pallas import tpu as pltpu
from jax.sharding import PartitionSpec as P

MESH = pl.DeviceIdType.MESH
epsilon = 1e-06
lambda_init = 0.8 - 0.6 * math.exp(-0.3)
bf16 = jnp.bfloat16
f32 = jnp.float32
HALO = 16
GROUP = 4
HUBS = (1, 2)
LANES = 128


def scope(name):
    return contextlib.nullcontext()


def parts_of(units):
    chunks = units // LANES
    first = (chunks + 1) // 2
    return ((0, first * LANES), (first * LANES, (chunks - first) * LANES))


def kernel(
    S, T, heads, dh, dv,
    q_hbm, kv_hbm, res_hbm, wout_hbm, wg_hbm, wu_hbm, wd_hbm,
    lam_ref, sub_ref, norm_ref, cg_ref, cu_ref,
    out_ref,
    q, kv, res, wout, wg, wu, wd, stage,
    m_s, l_s, acc_s, n_own, n_in, part, part_in, mid, hn,
    g_s, u_s, halo_out, halo_in, hid, low, low_in, half, half_in, done, ret,
    local_sem, own_sem, pair_sem, kv_send, kv_recv,
    w_send, w_recv, cross_send, stage_recv, stage_send, relay_send,
    tp_send, tp_recv, hn_send, hn_recv, ag_send, ag_recv,
    halo_send, halo_recv, core_send, core_recv, far_send, far_recv, ret_send, ret_recv,
):
    Z = S // 2
    sp = lax.axis_index("sp")
    tp = lax.axis_index("tp")
    z = lax.div(sp, 2)
    y = lax.rem(sp, 2)
    zi = lax.rem(z, GROUP)
    base = z - zi
    rows = q.shape[1]
    feat, units = wg_hbm.shape
    hh = heads // 2
    kw = 2 * hh * dh
    D = wout.shape[1]
    own = rows // T
    cap = wg.shape[1]
    pieces = parts_of(units)
    other = 1 - y
    mate = z * 2 + other
    has_up = z < Z - 1
    hub = (zi == HUBS[0]) | (zi == HUBS[1])
    near = jnp.where(zi == HUBS[0], z - 1, z + 1)
    core_mate = tp + 1 - 2 * lax.rem(tp, 2)
    far_mate = lax.rem(tp + 2, T)
    diagonal = T - 1 - tp

    def one(flag):
        return flag.astype(jnp.int32)

    def peer(d):
        return lax.rem(tp + d, T)

    def remote(src, dst, send, recv, device):
        return pltpu.make_async_remote_copy(
            src_ref=src, dst_ref=dst, send_sem=send, recv_sem=recv, device_id=device, device_id_type=MESH
        )

    def cols(k):
        return pl.ds(pieces[k][0], pieces[k][1])

    def block(b, k):
        return (pl.ds(pl.multiple_of(b * feat, feat), feat), pl.ds(0, pieces[k][1]))

    sources, stores = (wg_hbm, wu_hbm), (wg, wu)
    targets = [(g * GROUP + HUBS[k], k) for g in range(Z // GROUP) for k in range(2)]

    def direct(i, w):
        h, k = targets[i]
        return remote(
            sources[w].at[:, cols(k)], stores[w].at[block(sp, k)],
            w_send.at[w, i], w_recv.at[w, sp], (h * 2 + y, tp),
        )

    def cross(k, w):
        return remote(
            sources[w].at[:, cols(k)], stores[w].at[block(sp, k)],
            cross_send.at[w], w_recv.at[w, sp], (mate, tp),
        )

    def lend(k, w):
        return remote(
            sources[w].at[:, cols(k)], stage.at[w, :, pl.ds(0, pieces[k][1])],
            cross_send.at[w], stage_recv.at[w], (mate, tp),
        )

    def pass_on(k, w):
        h = base + HUBS[k]
        return remote(
            stage.at[w, :, pl.ds(0, pieces[k][1])], stores[w].at[block(mate, k)],
            stage_send.at[w], w_recv.at[w, mate], (h * 2 + y, tp),
        )

    def relay(zz, k, w):
        b = zz * 2 + y
        return remote(
            stores[w].at[block(b, k)], stores[w].at[block(b, k)],
            relay_send.at[w, zz], w_recv.at[w, b], (mate, tp),
        )

    def own_piece(k, w):
        return pltpu.make_async_copy(sources[w].at[:, cols(k)], stores[w].at[block(sp, k)], own_sem.at[w])

    def down_piece(k):
        return pltpu.make_async_copy(
            wd_hbm.at[cols(k), :], wd.at[pl.ds(0, pieces[k][1]), :], own_sem.at[2]
        )

    def as_hub(fn):
        for k in range(2):
            pl.when(zi == HUBS[k])(functools.partial(fn, k))

    def as_outer(fn):
        for k, zo in ((0, 0), (1, 3)):
            pl.when(zi == zo)(functools.partial(fn, k))

    loads = [
        pltpu.make_async_copy(kv_hbm.at[y], kv.at[sp], local_sem.at[0]),
        pltpu.make_async_copy(q_hbm.at[y], q.at[y], local_sem.at[1]),
        pltpu.make_async_copy(wout_hbm, wout, local_sem.at[2]),
        pltpu.make_async_copy(res_hbm.at[pl.ds(pl.multiple_of(tp * own, own), own), :], res, local_sem.at[3]),
    ]
    for c in loads:
        c.start()

    def load_pieces(k):
        own_piece(k, 0).start()
        own_piece(k, 1).start()
        down_piece(k).start()

    as_hub(load_pieces)

    barrier = pltpu.get_barrier_semaphore()
    next_group, prev_group = (y == 1) & (z + GROUP < Z), (y == 0) & (z >= GROUP)

    def greet(device):
        pl.semaphore_signal(barrier, inc=1, device_id=device, device_id_type=MESH)

    with scope("barrier"):
        for zz in range(Z):
            pl.when(z != zz)(functools.partial(greet, (zz * 2 + y, tp)))
        greet((mate, tp))
        for d in range(1, T):
            greet((sp, peer(d)))
        pl.when(next_group)(lambda: greet((sp + 2 * GROUP - 1, tp)))
        pl.when(prev_group)(lambda: greet((sp - 2 * GROUP + 1, tp)))
        pl.semaphore_wait(barrier, Z + T - 1 + one(next_group) + one(prev_group))

    def climb(blk):
        return remote(kv.at[blk], kv.at[blk], kv_send.at[blk], kv_recv.at[blk], (sp + 2, tp))

    def send_up(blk):
        pl.when(has_up)(lambda: climb(blk).start())

    def pair(src, dst, k):
        return remote(src, dst, pair_sem.at[0, k], pair_sem.at[1, k], (mate, tp))

    kv_swap = pair(kv_hbm.at[other], kv.at[sp], 0)
    q_swap = pair(q_hbm.at[other], q.at[y], 1)
    kv_got = pair(kv_hbm.at[other], kv.at[mate], 0)
    q_got = pair(q_hbm.at[other], q.at[other], 1)
    kv_swap.start()
    q_swap.start()
    loads[0].wait()
    send_up(sp)

    def direct_send(i):
        direct(i, 0).start()
        direct(i, 1).start()

    for i in reversed(range(len(targets))):
        pl.when(z > targets[i][0])(functools.partial(direct_send, i))

    def early(h):
        return (zi == 0) & (h == z + 1)

    for i in range(len(targets)):
        pl.when(early(targets[i][0]))(lambda: direct(i, 0).start())

    def cross_start(k):
        cross(k, 0).start()
        cross(k, 1).start()

    def lend_start(k):
        lend(k, 0).start()
        lend(k, 1).start()

    as_hub(cross_start)
    as_outer(lend_start)

    def forward_staged(k):
        for w in range(2):
            lend(k, w).wait_recv()
            pass_on(k, w).start()

    loads[1].wait()

    m_s[...] = jnp.full(m_s.shape, -1e30, f32)
    l_s[...] = jnp.zeros(l_s.shape, f32)
    acc_s[...] = jnp.zeros(acc_s.shape, f32)
    scale = 1.0 / math.sqrt(dh)

    def clear_tail(k):
        lo, wide = pieces[k][1], cap - pieces[k][1]
        if wide:
            wg[:, lo:] = jnp.zeros((D, wide), bf16)
            wu[:, lo:] = jnp.zeros((D, wide), bf16)
            wd[lo:, :] = jnp.zeros((wide, D), bf16)

    as_hub(clear_tail)

    def attend(yy, blk):
        row_at = (z * 2 + yy) * rows + lax.broadcasted_iota(jnp.int32, (rows, rows), 0)
        col_at = blk * rows + lax.broadcasted_iota(jnp.int32, (rows, rows), 1)
        keep = col_at <= row_at
        for h in range(hh):
            v = kv[blk, :, kw + h * dv : kw + (h + 1) * dv]
            for c in range(2):
                i = 2 * h + c
                k = kv[blk, :, i * dh : (i + 1) * dh]
                s = lax.dot_general(
                    q[yy, :, i * dh : (i + 1) * dh], k, (((1,), (1,)), ((), ())),
                    preferred_element_type=f32,
                ) * scale
                s = jnp.where(keep, s, -1e30)
                old = m_s[yy, i]
                new = jnp.maximum(old, jnp.max(s, axis=1, keepdims=True))
                e = jnp.where(keep, jnp.exp(s - new), 0.0)
                fade = jnp.exp(old - new)
                m_s[yy, i] = new
                l_s[yy, i] = l_s[yy, i] * fade + jnp.sum(e, axis=1, keepdims=True)
                acc_s[yy, i] = acc_s[yy, i] * fade + jnp.dot(
                    e.astype(bf16), v, preferred_element_type=f32
                )

    with scope("kvgot"):
        kv_got.wait_recv()
        send_up(mate)
        q_got.wait_recv()

    @pl.loop(0, Z)
    def _(r):
        @pl.when(z >= r)
        def _():
            @pl.when(r > 0)
            def _():
                for blk in (sp - 2 * r, mate - 2 * r):
                    with scope("arrkv"):
                        climb(blk).wait_recv()
                    send_up(blk)

            @pl.loop(0, 4)
            def _(i):
                yy, c = lax.div(i, 2), lax.rem(i, 2)
                with scope("attend"):
                    pl.when((r > 0) | (yy >= c))(lambda: attend(yy, (z - r) * 2 + c))

            pl.when((r == 2) & (zi == 3))(lambda: forward_staged(1))

    for i in range(len(targets)):
        h = targets[i][0]
        pl.when((z < h) & jnp.logical_not(early(h)))(lambda: direct(i, 0).start())
        pl.when(z < h)(lambda: direct(i, 1).start())

    def relayed(zz):
        return (zz != z) & (zz != near)

    def relay_from(zz):
        @pl.when(relayed(zz))
        def _():
            def go(k):
                for w in range(2):
                    relay(zz, k, w).wait_recv()
                    relay(zz, k, w).start()

            as_hub(go)

    with scope("nnorm"):
        for yy in range(2):
            for h in range(hh):
                a0 = acc_s[yy, 2 * h] / l_s[yy, 2 * h]
                a1 = acc_s[yy, 2 * h + 1] / l_s[yy, 2 * h + 1]
                a = a0 - lam_ref[y * hh + h] * a1
                ms = jnp.mean(a * a, axis=1, keepdims=True)
                n = a * lax.rsqrt(ms + epsilon) * sub_ref[...] * (1.0 - lambda_init)
                n_own[yy, :, h * dv : (h + 1) * dv] = n.astype(bf16)
    n_swap = pair(n_own.at[other], n_in, 2)
    n_swap.start()
    with scope("relay1"):
        pl.when(zi == HUBS[0])(lambda: relay_from(z + 1))
    with scope("nswapw"):
        loads[2].wait()
        n_swap.wait_recv()
    width = min(512, D)
    hw = hh * dv
    with scope("outproj"):
        for c in range(0, D, width):
            at = slice(c, c + width)
            part[:, :, at] = (
                (
                    jnp.dot(n_own[y], wout[pl.ds(y * hw, hw), at], preferred_element_type=f32)
                    + jnp.dot(n_in[...], wout[pl.ds(other * hw, hw), at], preferred_element_type=f32)
                )
                .astype(bf16)
                .reshape(T, own, width)
            )

    def swap(d):
        return remote(part.at[peer(d)], part_in.at[d], tp_send.at[d], tp_recv.at[d], (sp, peer(d)))

    firsts = [swap(d) for d in range(1, T)]
    for c in firsts:
        c.start()
    with scope("rs1"):
        loads[3].wait()
        total = res[...].astype(f32) + part[tp].astype(f32)
        for d in range(1, T):
            firsts[d - 1].wait_recv()
            total = total + part_in[d].astype(f32)
        mid[...] = total
        ms = jnp.mean(total * total, axis=1, keepdims=True)

    def slot(p, t):
        return hn.at[p, pl.ds(pl.multiple_of(t * own, own), own)]

    hn[zi, pl.ds(pl.multiple_of(tp * own, own), own), :] = (
        total * lax.rsqrt(ms + epsilon) * norm_ref[...]
    ).astype(bf16)

    def deliver(k):
        return remote(
            slot(zi, tp), slot(zi, tp), hn_send.at[k], hn_recv.at[zi], ((base + HUBS[k]) * 2 + y, tp)
        )

    pl.when(zi < 2)(lambda: deliver(1).start())
    pl.when(zi != HUBS[0])(lambda: deliver(0).start())
    pl.when(zi == 3)(lambda: deliver(1).start())
    pl.when(zi == 0)(lambda: forward_staged(0))

    with scope("relay2"):
        pl.when(zi == HUBS[0])(lambda: pl.loop(z + 2, Z)(relay_from))
        pl.when(zi == HUBS[1])(lambda: pl.loop(z + 2, Z)(relay_from))

        @pl.when(hub)
        def _():
            @pl.loop(0, z)
            def _(i):
                relay_from(z - 1 - i)

    def spread(p, hop):
        src = (tp, tp, far_mate)[hop]
        to = (far_mate, core_mate, core_mate)[hop]
        return remote(slot(p, src), slot(p, src), ag_send.at[p, hop], ag_recv.at[p, hop], (sp, to))

    def gather1(p):
        @pl.when(p != zi)
        def _():
            remote(slot(p, tp), slot(p, tp), hn_send.at[0], hn_recv.at[p], (sp, tp)).wait_recv()

        spread(p, 0).start()
        spread(p, 1).start()

    def gather2(p):
        spread(p, 0).wait_recv()
        spread(p, 2).start()

    def halo_copy(p):
        last = (y == 1) & (p == GROUP - 1)
        to = jnp.where(last, sp + 2 * GROUP - 1, mate)
        nxt = jnp.where(last, 0, p + y)
        return remote(
            halo_out.at[p], halo_in.at[nxt], halo_send.at[p], halo_recv.at[nxt], (to, tp)
        )

    def halo_sends(p):
        return (y == 0) | (p < GROUP - 1) | (z + GROUP < Z)

    def core_copy(p, i):
        return remote(
            low.at[p, (core_mate, diagonal)[i]], low_in.at[p, i], core_send.at[p, i], core_recv.at[p, i],
            (sp, core_mate),
        )

    def far_copy(p):
        return remote(half.at[p], half_in.at[p], far_send.at[p], far_recv.at[p], (sp, far_mate))

    def give_back(p, k):
        return remote(done.at[p], ret.at[k], ret_send.at[p], ret_recv.at[k], ((base + p) * 2 + y, tp))

    def feed(p):
        wide = 256
        for c in range(0, cap, wide):
            at = slice(c, c + wide)
            g_s[HALO:, at] = jnp.dot(hn[p], wg[:, at], preferred_element_type=f32).astype(bf16).astype(f32)
            u_s[HALO:, at] = jnp.dot(hn[p], wu[:, at], preferred_element_type=f32).astype(bf16).astype(f32)
        halo_out[p, 0] = g_s[rows:, :].astype(bf16)
        halo_out[p, 1] = u_s[rows:, :].astype(bf16)
        pl.when(halo_sends(p))(lambda: halo_copy(p).start())
        first = (y == 0) & (p == 0) & (base == 0)

        @pl.when(first)
        def _():
            g_s[:HALO, :] = jnp.zeros((HALO, cap), f32)
            u_s[:HALO, :] = jnp.zeros((HALO, cap), f32)

        @pl.when(jnp.logical_not(first))
        def _():
            remote(halo_out.at[p], halo_in.at[p], halo_send.at[p], halo_recv.at[p], (mate, tp)).wait_recv()
            g_s[:HALO, :] = halo_in[p, 0].astype(f32)
            u_s[:HALO, :] = halo_in[p, 1].astype(f32)

        lo = jnp.where(zi == HUBS[0], pieces[0][0], pieces[1][0])
        for c in range(0, cap, LANES):
            at = slice(c, c + LANES)
            tap = pl.ds(pl.multiple_of(jnp.minimum(lo + c, units - LANES), LANES), LANES)

            def mix(x, taps):
                out = taps[0:1, tap] * x[HALO - 2 : HALO - 2 + rows, at]
                out = out + taps[1:2, tap] * x[HALO - 1 : HALO - 1 + rows, at]
                return out + taps[2:3, tap] * x[HALO:, at]

            gm, um = mix(g_s, cg_ref), mix(u_s, cu_ref)
            hid[:, at] = (gm / (1.0 + jnp.exp(-gm)) * um).astype(bf16)
        for c in range(0, D, width):
            at = slice(c, c + width)
            low[p, :, :, at] = (
                jnp.dot(hid[...], wd[:, at], preferred_element_type=f32).astype(bf16).reshape(T, own, width)
            )
        core_copy(p, 1).start()
        core_copy(p, 0).start()

    def reduce1(p):
        core_copy(p, 1).wait_recv()
        half[p] = (low[p, far_mate].astype(f32) + low_in[p, 1].astype(f32)).astype(bf16)
        far_copy(p).start()

    def reduce2(p):
        core_copy(p, 0).wait_recv()
        far_copy(p).wait_recv()
        t = low[p, tp].astype(f32) + low_in[p, 0].astype(f32) + half_in[p].astype(f32)

        def hand(k):
            @pl.when(p == zi)
            def _():
                ret[k] = t.astype(bf16)

            @pl.when(p != zi)
            def _():
                done[p] = t.astype(bf16)
                give_back(p, k).start()

        as_hub(hand)

    def wait_pieces(k):
        for w in range(2):
            own_piece(k, w).wait()

            def arrived(b):
                remote(
                    stores[w].at[block(b, k)], stores[w].at[block(b, k)],
                    cross_send.at[w], w_recv.at[w, b], (mate, tp),
                ).wait_recv()

            arrived(near * 2 + y)

            @pl.loop(0, Z)
            def _(zz):
                arrived(zz * 2 + other)

        down_piece(k).wait()

    @pl.when(hub)
    def _():
        with scope("gather"):
            for p in range(3):
                gather1(p)
                gather2(p)

        with scope("wwait"):
            as_hub(wait_pieces)

        @pl.loop(0, GROUP)
        def _(p):
            @pl.when(p == GROUP - 2)
            def _():
                with scope("gather3"):
                    gather1(GROUP - 1)

            @pl.when(p == GROUP - 1)
            def _():
                with scope("gather4"):
                    gather2(GROUP - 1)

            with scope("agw"):
                spread(p, 1).wait_recv()
                spread(p, 2).wait_recv()
            with scope("feed"):
                feed(p)

            @pl.when((p > 0) & (p < GROUP - 1))
            def _():
                with scope("red"):
                    reduce1(p - 1)

        with scope("redlast"):
            reduce1(GROUP - 2)
            reduce2(0)
            reduce1(GROUP - 1)
            for p in range(1, GROUP):
                reduce2(p)

    with scope("final"):
        total = mid[...]
        for k in range(2):
            pl.when(zi != HUBS[k])(
                lambda: remote(done.at[0], ret.at[k], ret_send.at[0], ret_recv.at[k], (sp, tp)).wait_recv()
            )
            total = total + ret[k].astype(f32)
        out_ref[...] = total.astype(bf16)

    with scope("drain"):
        @pl.loop(0, Z)
        def _(zz):
            @pl.when(has_up & (zz <= z))
            def _():
                climb(2 * zz).wait_send()
                climb(2 * zz + 1).wait_send()

            @pl.when(hub & relayed(zz))
            def _():
                def go(k):
                    relay(zz, k, 0).wait_send()
                    relay(zz, k, 1).wait_send()

                as_hub(go)

        for i in range(len(targets)):
            @pl.when(z != targets[i][0])
            def _():
                direct(i, 0).wait_send()
                direct(i, 1).wait_send()

        def cross_end(k):
            cross(k, 0).wait_send()
            cross(k, 1).wait_send()

        def lend_end(k):
            for w in range(2):
                lend(k, w).wait_send()
                pass_on(k, w).wait_send()

        as_hub(cross_end)
        as_outer(lend_end)
        for c in firsts + [kv_swap, q_swap, n_swap]:
            c.wait_send()
        for k in range(2):
            pl.when(zi != HUBS[k])(lambda: deliver(k).wait_send())

        @pl.when(hub)
        def _():
            @pl.loop(0, GROUP)
            def _(p):
                for hop in range(3):
                    spread(p, hop).wait_send()
                pl.when(halo_sends(p))(lambda: halo_copy(p).wait_send())
                core_copy(p, 0).wait_send()
                core_copy(p, 1).wait_send()
                far_copy(p).wait_send()
                pl.when(p != zi)(lambda: give_back(p, 0).wait_send())


def local(
    S, T,
    residual, queries, key_rows, values, lambda_head, sub_gain, w_out, norm_gain,
    w_gate, w_up, conv_gate, conv_up, w_down,
):
    rows, heads, maps, dh = queries.shape
    dv = values.shape[2]
    feat, units = w_gate.shape
    D = w_out.shape[1]
    own = rows // T
    cap = max(p[1] for p in parts_of(units))
    hh = heads // 2
    q = queries.reshape(rows, 2, hh * maps * dh).swapaxes(0, 1)
    kv = jnp.concatenate(
        [key_rows.reshape(rows, 2, hh * maps * dh), values.reshape(rows, 2, hh * dv)], axis=2
    ).swapaxes(0, 1)
    kvw = kv.shape[2]
    Z = S // 2
    hbm = pl.BlockSpec(memory_space=pl.ANY)
    vmem = pl.BlockSpec(memory_space=pltpu.VMEM)
    smem = pl.BlockSpec(memory_space=pltpu.SMEM)
    V = pltpu.VMEM
    dma = pltpu.SemaphoreType.DMA
    return pl.pallas_call(
        functools.partial(kernel, S, T, heads, dh, dv),
        out_shape=jax.ShapeDtypeStruct((own, D), bf16),
        in_specs=[hbm] * 7 + [smem] + [vmem] * 4,
        out_specs=vmem,
        scratch_shapes=[
            V(q.shape, bf16),
            V((S, rows, kvw), bf16),
            V((own, D), bf16),
            V(w_out.shape, bf16),
            V((D, cap), bf16),
            V((D, cap), bf16),
            V((cap, D), bf16),
            V((2, feat, cap), bf16),
            V((2, 2 * hh, rows, 1), f32),
            V((2, 2 * hh, rows, 1), f32),
            V((2, 2 * hh, rows, dv), f32),
            V((2, rows, hh * dv), bf16),
            V((rows, hh * dv), bf16),
            V((T, own, D), bf16),
            V((T, own, D), bf16),
            V((own, D), f32),
            V((GROUP, rows, D), bf16),
            V((rows + HALO, cap), f32),
            V((rows + HALO, cap), f32),
            V((GROUP, 2, HALO, cap), bf16),
            V((GROUP, 2, HALO, cap), bf16),
            V((rows, cap), bf16),
            V((GROUP, T, own, D), bf16),
            V((GROUP, 2, own, D), bf16),
            V((GROUP, own, D), bf16),
            V((GROUP, own, D), bf16),
            V((GROUP, own, D), bf16),
            V((2, own, D), bf16),
            dma((4,)),
            dma((3,)),
            dma((2, 3)),
            dma((S,)),
            dma((S,)),
            dma((2, Z // 2)),
            dma((2, S)),
            dma((2,)),
            dma((2,)),
            dma((2,)),
            dma((2, Z)),
            dma((T,)),
            dma((T,)),
            dma((2,)),
            dma((GROUP,)),
            dma((GROUP, 3)),
            dma((GROUP, 3)),
            dma((GROUP,)),
            dma((GROUP,)),
            dma((GROUP, 2)),
            dma((GROUP, 2)),
            dma((GROUP,)),
            dma((GROUP,)),
            dma((GROUP,)),
            dma((2,)),
        ],
        compiler_params=pltpu.CompilerParams(
            collective_id=0, has_side_effects=True, vmem_limit_bytes=64000000
        ),
    )(
        q, kv, residual, w_out, w_gate, w_up, w_down, lambda_head,
        sub_gain.reshape(1, -1), norm_gain.reshape(1, -1), conv_gate, conv_up,
    )


def solution(mesh):
    placed = (
        P("sp", None),
        P("sp", "tp", None, None),
        P("sp", "tp", None, None),
        P("sp", "tp", None),
        P("tp"),
        P(),
        P("tp", None),
        P(),
        P("sp", "tp"),
        P("sp", "tp"),
        P(None, "tp"),
        P(None, "tp"),
        P("tp", None),
    )
    return jax.shard_map(
        functools.partial(local, mesh.shape["sp"], mesh.shape["tp"]),
        mesh=mesh, in_specs=placed, out_specs=P(("sp", "tp"), None), check_vma=False,
    )
```

time: 176 us -> 144 us (0.82)
  Pallas kernels: 168 us -> 137 us
    pallas_call x1, Pallas kernels: 168 us -> 137 us  [local(): pl.pallas_call(functools.partial(kernel, S, T, heads, dh, dv), out_shape=...]
where the time goes in v1:
time: 144 us; the launch traced here: 143 us
  Pallas kernels  137 us (95%)
  local copies, waits for them, and re-layouts  5.65 us (4%)
    pallas_call x1, Pallas kernels, local(): pl.pallas_call(functools.partial(kernel, S, T, heads, dh, dv), out_shape=...  137 us

profile of v1, /device:TPU:29, one launch (start us, length us, event | category | flops | bytes accessed | tf_op | source)
XLA Modules:
  0.0 143.3 jit_solution(3437500538300245476)
XLA Ops:
  0.0 1.1 reshape.17
  1.2 1.0 copy.16
  2.1 0.8 maximum_bitcast_fusion.kv_hbm
  3.0 1.1 reshape.16
  4.1 0.7 copy.20
  4.8 136.8 %shard_map.127 = bf16[64,2048]{1,0:T(8,128)(2,1)} custom-call(bf16[2,256,256]{2,1,0:T(8,128)(2,1)} %bitcast.7, bf16[2,256,512]{2,1,0:T(8,128)(2,1)} %maximum_bitcast_fusion.kv_hbm, bf16[256,2048]{1,0:T(8,128)(2,1)} %res_hbm.1, bf16[512,2048]{1,0:T(8,128)(2,1)} %wout_hbm.1, bf16[256,1408]{1,0:T(8,128)(2,1)} %wg_hbm.1, bf16[256,1408]{1,0:T(8,128)(2,1)} %wu_hbm.1, ...), custom_call_target="tpu_custom_call" | custom-call | tf_op jit(solution)/shard_map/pallas_call | solution.py:617
  141.7 1.7 %copy.22 = bf16[64,2048]{1,0:T(8,128)(2,1)} copy(bf16[64,2048]{1,0:T(8,128)(2,1)} %shard_map.127) | data formatting | bytes 524288
  (1 shorter events, 0.0 us)

commit v2 on v1

--- a/solution.py
+++ b/solution.py
@@ -18,6 +18,8 @@
 GROUP = 4
 HUBS = (1, 2)
 LANES = 128
+SPLIT = 2
+STAGED = {3: ((1, 0), (0, 0), (0, 1))}
 
 
 def scope(name):
@@ -32,14 +34,14 @@
 
 def kernel(
     S, T, heads, dh, dv,
-    q_hbm, kv_hbm, res_hbm, wout_hbm, wg_hbm, wu_hbm, wd_hbm,
+    q_hbm, k_hbm, v_hbm, res_hbm, wout_hbm, wg_hbm, wu_hbm, wd_hbm,
     lam_ref, sub_ref, norm_ref, cg_ref, cu_ref,
     out_ref,
-    q, kv, res, wout, wg, wu, wd, stage,
+    q_raw, k_raw, v_raw, q_out, kv_out, q, kv, res, wout, wg, wu, wd, stage,
     m_s, l_s, acc_s, n_own, n_in, part, part_in, mid, hn,
     g_s, u_s, halo_out, halo_in, hid, low, low_in, half, half_in, done, ret,
     local_sem, own_sem, pair_sem, kv_send, kv_recv,
-    w_send, w_recv, cross_send, stage_recv, stage_send, relay_send,
+    w_send, w_recv, cross_send, lend_send, stage_recv, stage_send, relay_send,
     tp_send, tp_recv, hn_send, hn_recv, ag_send, ag_recv,
     halo_send, halo_recv, core_send, core_recv, far_send, far_recv, ret_send, ret_recv,
 ):
@@ -62,7 +64,6 @@
     mate = z * 2 + other
     has_up = z < Z - 1
     hub = (zi == HUBS[0]) | (zi == HUBS[1])
-    near = jnp.where(zi == HUBS[0], z - 1, z + 1)
     core_mate = tp + 1 - 2 * lax.rem(tp, 2)
     far_mate = lax.rem(tp + 2, T)
     diagonal = T - 1 - tp
@@ -102,16 +103,28 @@
 
     def lend(k, w):
         return remote(
-            sources[w].at[:, cols(k)], stage.at[w, :, pl.ds(0, pieces[k][1])],
-            cross_send.at[w], stage_recv.at[w], (mate, tp),
+            sources[w].at[:, cols(k)], stage.at[k, w, :, pl.ds(0, pieces[k][1])],
+            lend_send.at[k, w], stage_recv.at[k, w], (mate, tp),
         )
 
     def pass_on(k, w):
         h = base + HUBS[k]
         return remote(
-            stage.at[w, :, pl.ds(0, pieces[k][1])], stores[w].at[block(mate, k)],
-            stage_send.at[w], w_recv.at[w, mate], (h * 2 + y, tp),
-        )
+            stage.at[k, w, :, pl.ds(0, pieces[k][1])], stores[w].at[block(mate, k)],
+            stage_send.at[k, w], w_recv.at[w, mate], (h * 2 + y, tp),
+        )
+
+    def staged(zz, k, w):
+        hit = zz < 0
+        for zo, which in STAGED.items():
+            if (k, w) in which:
+                hit = hit | (zz == base + zo)
+        return hit
+
+    def each_staged(fn):
+        for zo, which in STAGED.items():
+            for k, w in which:
+                pl.when(zi == zo)(functools.partial(fn, k, w))
 
     def relay(zz, k, w):
         b = zz * 2 + y
@@ -132,13 +145,10 @@
         for k in range(2):
             pl.when(zi == HUBS[k])(functools.partial(fn, k))
 
-    def as_outer(fn):
-        for k, zo in ((0, 0), (1, 3)):
-            pl.when(zi == zo)(functools.partial(fn, k))
-
     loads = [
-        pltpu.make_async_copy(kv_hbm.at[y], kv.at[sp], local_sem.at[0]),
-        pltpu.make_async_copy(q_hbm.at[y], q.at[y], local_sem.at[1]),
+        pltpu.make_async_copy(k_hbm, k_raw, local_sem.at[0]),
+        pltpu.make_async_copy(v_hbm, v_raw, local_sem.at[4]),
+        pltpu.make_async_copy(q_hbm, q_raw, local_sem.at[1]),
         pltpu.make_async_copy(wout_hbm, wout, local_sem.at[2]),
         pltpu.make_async_copy(res_hbm.at[pl.ds(pl.multiple_of(tp * own, own), own), :], res, local_sem.at[3]),
     ]
@@ -166,6 +176,20 @@
             greet((sp, peer(d)))
         pl.when(next_group)(lambda: greet((sp + 2 * GROUP - 1, tp)))
         pl.when(prev_group)(lambda: greet((sp - 2 * GROUP + 1, tp)))
+        with scope("relayout"):
+            for c in loads[:3]:
+                c.wait()
+            for yy in range(2):
+                @pl.when(y == yy)
+                def _():
+                    for mine, q_to, kv_to in ((True, q.at[y], kv.at[sp]), (False, q_out, kv_out)):
+                        for h in range(hh):
+                            head = (yy if mine else 1 - yy) * hh + h
+                            for c in range(2):
+                                i = 2 * h + c
+                                q_to[:, i * dh : (i + 1) * dh] = q_raw[:, head, c, :]
+                                kv_to[:, i * dh : (i + 1) * dh] = k_raw[:, head, c, :]
+                            kv_to[:, kw + h * dv : kw + (h + 1) * dv] = v_raw[:, head, :]
         pl.semaphore_wait(barrier, Z + T - 1 + one(next_group) + one(prev_group))
 
     def climb(blk):
@@ -177,13 +201,12 @@
     def pair(src, dst, k):
         return remote(src, dst, pair_sem.at[0, k], pair_sem.at[1, k], (mate, tp))
 
-    kv_swap = pair(kv_hbm.at[other], kv.at[sp], 0)
-    q_swap = pair(q_hbm.at[other], q.at[y], 1)
-    kv_got = pair(kv_hbm.at[other], kv.at[mate], 0)
-    q_got = pair(q_hbm.at[other], q.at[other], 1)
+    kv_swap = pair(kv_out, kv.at[sp], 0)
+    q_swap = pair(q_out, q.at[y], 1)
+    kv_got = pair(kv_out, kv.at[mate], 0)
+    q_got = pair(q_out, q.at[other], 1)
     kv_swap.start()
     q_swap.start()
-    loads[0].wait()
     send_up(sp)
 
     def direct_send(i):
@@ -194,7 +217,7 @@
         pl.when(z > targets[i][0])(functools.partial(direct_send, i))
 
     def early(h):
-        return (zi == 0) & (h == z + 1)
+        return (zi == 1) & (h == z + 1)
 
     for i in range(len(targets)):
         pl.when(early(targets[i][0]))(lambda: direct(i, 0).start())
@@ -203,19 +226,12 @@
         cross(k, 0).start()
         cross(k, 1).start()
 
-    def lend_start(k):
-        lend(k, 0).start()
-        lend(k, 1).start()
-
     as_hub(cross_start)
-    as_outer(lend_start)
-
-    def forward_staged(k):
-        for w in range(2):
-            lend(k, w).wait_recv()
-            pass_on(k, w).start()
-
-    loads[1].wait()
+    each_staged(lambda k, w: lend(k, w).start())
+
+    def forward(k, w):
+        lend(k, w).wait_recv()
+        pass_on(k, w).start()
 
     m_s[...] = jnp.full(m_s.shape, -1e30, f32)
     l_s[...] = jnp.zeros(l_s.shape, f32)
@@ -255,6 +271,19 @@
                     e.astype(bf16), v, preferred_element_type=f32
                 )
 
+    def late(h):
+        return (zi == 0) & (h > z + 1)
+
+    def relay_from(zz, w):
+        def go(k):
+            @pl.when((zz != z) & jnp.logical_not(staged(zz, k, w)))
+            def _():
+                with scope("rly"):
+                    relay(zz, k, w).wait_recv()
+                relay(zz, k, w).start()
+
+        as_hub(go)
+
     with scope("kvgot"):
         kv_got.wait_recv()
         send_up(mate)
@@ -277,25 +306,22 @@
                 with scope("attend"):
                     pl.when((r > 0) | (yy >= c))(lambda: attend(yy, (z - r) * 2 + c))
 
-            pl.when((r == 2) & (zi == 3))(lambda: forward_staged(1))
+            @pl.when((r == 1) & (zi == HUBS[1]))
+            def _():
+                relay_from(z - 1, 0)
+                relay_from(z + 1, 1)
+
+            @pl.when((r == 2) & (zi == 3))
+            def _():
+                forward(1, 0)
+                forward(0, 0)
+
+            pl.when((r == 3) & (zi == 3))(lambda: forward(0, 1))
 
     for i in range(len(targets)):
         h = targets[i][0]
-        pl.when((z < h) & jnp.logical_not(early(h)))(lambda: direct(i, 0).start())
-        pl.when(z < h)(lambda: direct(i, 1).start())
-
-    def relayed(zz):
-        return (zz != z) & (zz != near)
-
-    def relay_from(zz):
-        @pl.when(relayed(zz))
-        def _():
-            def go(k):
-                for w in range(2):
-                    relay(zz, k, w).wait_recv()
-                    relay(zz, k, w).start()
-
-            as_hub(go)
+        pl.when((z < h) & jnp.logical_not(early(h) | late(h)))(lambda: direct(i, 0).start())
+        pl.when((z < h) & jnp.logical_not(late(h)))(lambda: direct(i, 1).start())
 
     with scope("nnorm"):
         for yy in range(2):
@@ -309,9 +335,9 @@
     n_swap = pair(n_own.at[other], n_in, 2)
     n_swap.start()
     with scope("relay1"):
-        pl.when(zi == HUBS[0])(lambda: relay_from(z + 1))
+        pl.when(zi == HUBS[0])(lambda: relay_from(z + 1, 0))
     with scope("nswapw"):
-        loads[2].wait()
+        loads[3].wait()
         n_swap.wait_recv()
     width = min(512, D)
     hw = hh * dv
@@ -333,8 +359,11 @@
     firsts = [swap(d) for d in range(1, T)]
     for c in firsts:
         c.start()
+    twin = jnp.where(zi == HUBS[0], z + 1, z - 1)
+    with scope("relayt"):
+        pl.when(hub)(lambda: relay_from(twin, 1))
     with scope("rs1"):
-        loads[3].wait()
+        loads[4].wait()
         total = res[...].astype(f32) + part[tp].astype(f32)
         for d in range(1, T):
             firsts[d - 1].wait_recv()
@@ -354,20 +383,10 @@
             slot(zi, tp), slot(zi, tp), hn_send.at[k], hn_recv.at[zi], ((base + HUBS[k]) * 2 + y, tp)
         )
 
-    pl.when(zi < 2)(lambda: deliver(1).start())
     pl.when(zi != HUBS[0])(lambda: deliver(0).start())
-    pl.when(zi == 3)(lambda: deliver(1).start())
-    pl.when(zi == 0)(lambda: forward_staged(0))
-
-    with scope("relay2"):
-        pl.when(zi == HUBS[0])(lambda: pl.loop(z + 2, Z)(relay_from))
-        pl.when(zi == HUBS[1])(lambda: pl.loop(z + 2, Z)(relay_from))
-
-        @pl.when(hub)
-        def _():
-            @pl.loop(0, z)
-            def _(i):
-                relay_from(z - 1 - i)
+    pl.when(zi != HUBS[1])(lambda: deliver(1).start())
+    for i in range(len(targets)):
+        pl.when((z < targets[i][0]) & late(targets[i][0]))(functools.partial(direct_send, i))
 
     def spread(p, hop):
         src = (tp, tp, far_mate)[hop]
@@ -386,6 +405,20 @@
         spread(p, 0).wait_recv()
         spread(p, 2).start()
 
+    @pl.when(hub)
+    def _():
+        with scope("g1"):
+            gather1(zi)
+
+    with scope("relay2"):
+        @pl.when(hub)
+        def _():
+            for w in range(2):
+                @pl.loop(0, Z)
+                def _(i):
+                    done_before = (Z - 1 - i == twin) | ((zi == HUBS[1]) & (Z - 1 - i == z + 1))
+                    pl.when(jnp.logical_not(done_before))(lambda: relay_from(Z - 1 - i, w))
+
     def halo_copy(p):
         last = (y == 1) & (p == GROUP - 1)
         to = jnp.where(last, sp + 2 * GROUP - 1, mate)
@@ -397,17 +430,52 @@
     def halo_sends(p):
         return (y == 0) | (p < GROUP - 1) | (z + GROUP < Z)
 
-    def core_copy(p, i):
-        return remote(
-            low.at[p, (core_mate, diagonal)[i]], low_in.at[p, i], core_send.at[p, i], core_recv.at[p, i],
-            (sp, core_mate),
-        )
-
-    def far_copy(p):
-        return remote(half.at[p], half_in.at[p], far_send.at[p], far_recv.at[p], (sp, far_mate))
-
-    def give_back(p, k):
-        return remote(done.at[p], ret.at[k], ret_send.at[p], ret_recv.at[k], ((base + p) * 2 + y, tp))
+    side = D // SPLIT
+
+    def span(h):
+        return pl.ds(h * side, side)
+
+    def core_copy(p, i, h):
+        return remote(
+            low.at[p, (core_mate, diagonal)[i], :, span(h)], low_in.at[p, i, :, span(h)],
+            core_send.at[p, i, h], core_recv.at[p, i, h], (sp, core_mate),
+        )
+
+    def far_copy(p, h):
+        return remote(
+            half.at[p, :, span(h)], half_in.at[p, :, span(h)], far_send.at[p, h], far_recv.at[p, h],
+            (sp, far_mate),
+        )
+
+    def give_back(p, k, h):
+        return remote(
+            done.at[p, :, span(h)], ret.at[k, :, span(h)], ret_send.at[p, h], ret_recv.at[k, h],
+            ((base + p) * 2 + y, tp),
+        )
+
+    def reduce1(p, h):
+        core_copy(p, 1, h).wait_recv()
+        at = slice(h * side, (h + 1) * side)
+        half[p, :, at] = (low[p, far_mate, :, at].astype(f32) + low_in[p, 1, :, at].astype(f32)).astype(bf16)
+        far_copy(p, h).start()
+
+    def reduce2(p, h):
+        core_copy(p, 0, h).wait_recv()
+        far_copy(p, h).wait_recv()
+        at = slice(h * side, (h + 1) * side)
+        t = low[p, tp, :, at].astype(f32) + low_in[p, 0, :, at].astype(f32) + half_in[p, :, at].astype(f32)
+
+        def hand(k):
+            @pl.when(p == zi)
+            def _():
+                ret[k, :, at] = t.astype(bf16)
+
+            @pl.when(p != zi)
+            def _():
+                done[p, :, at] = t.astype(bf16)
+                give_back(p, k, h).start()
+
+        as_hub(hand)
 
     def feed(p):
         wide = 256
@@ -418,6 +486,12 @@
         halo_out[p, 0] = g_s[rows:, :].astype(bf16)
         halo_out[p, 1] = u_s[rows:, :].astype(bf16)
         pl.when(halo_sends(p))(lambda: halo_copy(p).start())
+
+        @pl.when(p > 0)
+        def _():
+            for h in range(SPLIT):
+                reduce1(p - 1, h)
+
         first = (y == 0) & (p == 0) & (base == 0)
 
         @pl.when(first)
@@ -448,67 +522,54 @@
             low[p, :, :, at] = (
                 jnp.dot(hid[...], wd[:, at], preferred_element_type=f32).astype(bf16).reshape(T, own, width)
             )
-        core_copy(p, 1).start()
-        core_copy(p, 0).start()
-
-    def reduce1(p):
-        core_copy(p, 1).wait_recv()
-        half[p] = (low[p, far_mate].astype(f32) + low_in[p, 1].astype(f32)).astype(bf16)
-        far_copy(p).start()
-
-    def reduce2(p):
-        core_copy(p, 0).wait_recv()
-        far_copy(p).wait_recv()
-        t = low[p, tp].astype(f32) + low_in[p, 0].astype(f32) + half_in[p].astype(f32)
-
-        def hand(k):
-            @pl.when(p == zi)
-            def _():
-                ret[k] = t.astype(bf16)
-
-            @pl.when(p != zi)
-            def _():
-                done[p] = t.astype(bf16)
-                give_back(p, k).start()
-
-        as_hub(hand)
+            if (c + width) % side == 0:
+                core_copy(p, 1, c // side).start()
+                core_copy(p, 0, c // side).start()
 
     def wait_pieces(k):
         for w in range(2):
             own_piece(k, w).wait()
 
             def arrived(b):
+              with scope("arrw"):
                 remote(
                     stores[w].at[block(b, k)], stores[w].at[block(b, k)],
                     cross_send.at[w], w_recv.at[w, b], (mate, tp),
                 ).wait_recv()
 
-            arrived(near * 2 + y)
-
             @pl.loop(0, Z)
             def _(zz):
+                pl.when(staged(zz, k, w))(lambda: arrived(zz * 2 + y))
                 arrived(zz * 2 + other)
 
         down_piece(k).wait()
 
     @pl.when(hub)
     def _():
-        with scope("gather"):
-            for p in range(3):
-                gather1(p)
-                gather2(p)
+        with scope("ga"):
+            pl.when(zi != HUBS[0])(lambda: gather1(HUBS[0]))
+            gather1(0)
+            gather2(zi)
+            pl.when(zi != HUBS[0])(lambda: gather2(HUBS[0]))
+            pl.when(zi != HUBS[1])(lambda: gather1(HUBS[1]))
+            gather2(0)
 
         with scope("wwait"):
             as_hub(wait_pieces)
 
         @pl.loop(0, GROUP)
         def _(p):
-            @pl.when(p == GROUP - 2)
+            @pl.when(p == 0)
+            def _():
+                with scope("gather2"):
+                    gather1(GROUP - 1)
+
+            @pl.when(p == 1)
             def _():
                 with scope("gather3"):
-                    gather1(GROUP - 1)
-
-            @pl.when(p == GROUP - 1)
+                    pl.when(zi != HUBS[1])(lambda: gather2(HUBS[1]))
+
+            @pl.when(p == 2)
             def _():
                 with scope("gather4"):
                     gather2(GROUP - 1)
@@ -519,26 +580,26 @@
             with scope("feed"):
                 feed(p)
 
-            @pl.when((p > 0) & (p < GROUP - 1))
-            def _():
-                with scope("red"):
-                    reduce1(p - 1)
-
         with scope("redlast"):
-            reduce1(GROUP - 2)
-            reduce2(0)
-            reduce1(GROUP - 1)
-            for p in range(1, GROUP):
-                reduce2(p)
+            for h in range(SPLIT):
+                with scope("r13"):
+                    reduce1(GROUP - 1, h)
+            for p in range(GROUP):
+                for h in range(SPLIT):
+                    with scope(f"r2{p}{h}"):
+                        reduce2(p, h)
 
     with scope("final"):
-        total = mid[...]
-        for k in range(2):
-            pl.when(zi != HUBS[k])(
-                lambda: remote(done.at[0], ret.at[k], ret_send.at[0], ret_recv.at[k], (sp, tp)).wait_recv()
-            )
-            total = total + ret[k].astype(f32)
-        out_ref[...] = total.astype(bf16)
+        for h in range(SPLIT):
+            at = slice(h * side, (h + 1) * side)
+            total = mid[:, at]
+            for k in range(2):
+                got = remote(
+                    done.at[0, :, span(h)], ret.at[k, :, span(h)], ret_send.at[0, h], ret_recv.at[k, h], (sp, tp)
+                )
+                pl.when(zi != HUBS[k])(got.wait_recv)
+                total = total + ret[k, :, at].astype(f32)
+            out_ref[:, at] = total.astype(bf16)
 
     with scope("drain"):
         @pl.loop(0, Z)
@@ -548,13 +609,11 @@
                 climb(2 * zz).wait_send()
                 climb(2 * zz + 1).wait_send()
 
-            @pl.when(hub & relayed(zz))
-            def _():
-                def go(k):
-                    relay(zz, k, 0).wait_send()
-                    relay(zz, k, 1).wait_send()
-
-                as_hub(go)
+            def go(k):
+                for w in range(2):
+                    pl.when((zz != z) & jnp.logical_not(staged(zz, k, w)))(relay(zz, k, w).wait_send)
+
+            as_hub(go)
 
         for i in range(len(targets)):
             @pl.when(z != targets[i][0])
@@ -566,13 +625,13 @@
             cross(k, 0).wait_send()
             cross(k, 1).wait_send()
 
-        def lend_end(k):
-            for w in range(2):
-                lend(k, w).wait_send()
-                pass_on(k, w).wait_send()
-
         as_hub(cross_end)
-        as_outer(lend_end)
+
+        def lend_end(k, w):
+            lend(k, w).wait_send()
+            pass_on(k, w).wait_send()
+
+        each_staged(lend_end)
         for c in firsts + [kv_swap, q_swap, n_swap]:
             c.wait_send()
         for k in range(2):
@@ -585,10 +644,11 @@
                 for hop in range(3):
                     spread(p, hop).wait_send()
                 pl.when(halo_sends(p))(lambda: halo_copy(p).wait_send())
-                core_copy(p, 0).wait_send()
-                core_copy(p, 1).wait_send()
-                far_copy(p).wait_send()
-                pl.when(p != zi)(lambda: give_back(p, 0).wait_send())
+                for h in range(SPLIT):
+                    core_copy(p, 0, h).wait_send()
+                    core_copy(p, 1, h).wait_send()
+                    far_copy(p, h).wait_send()
+                    pl.when(p != zi)(give_back(p, 0, h).wait_send)
 
 
 def local(
@@ -603,11 +663,8 @@
     own = rows // T
     cap = max(p[1] for p in parts_of(units))
     hh = heads // 2
-    q = queries.reshape(rows, 2, hh * maps * dh).swapaxes(0, 1)
-    kv = jnp.concatenate(
-        [key_rows.reshape(rows, 2, hh * maps * dh), values.reshape(rows, 2, hh * dv)], axis=2
-    ).swapaxes(0, 1)
-    kvw = kv.shape[2]
+    qw = hh * maps * dh
+    kvw = qw + hh * dv
     Z = S // 2
     hbm = pl.BlockSpec(memory_space=pl.ANY)
     vmem = pl.BlockSpec(memory_space=pltpu.VMEM)
@@ -617,17 +674,22 @@
     return pl.pallas_call(
         functools.partial(kernel, S, T, heads, dh, dv),
         out_shape=jax.ShapeDtypeStruct((own, D), bf16),
-        in_specs=[hbm] * 7 + [smem] + [vmem] * 4,
+        in_specs=[hbm] * 8 + [smem] + [vmem] * 4,
         out_specs=vmem,
         scratch_shapes=[
-            V(q.shape, bf16),
+            V(queries.shape, bf16),
+            V(key_rows.shape, bf16),
+            V(values.shape, bf16),
+            V((rows, qw), bf16),
+            V((rows, kvw), bf16),
+            V((2, rows, qw), bf16),
             V((S, rows, kvw), bf16),
             V((own, D), bf16),
             V(w_out.shape, bf16),
             V((D, cap), bf16),
             V((D, cap), bf16),
             V((cap, D), bf16),
-            V((2, feat, cap), bf16),
+            V((2, 2, feat, cap), bf16),
             V((2, 2 * hh, rows, 1), f32),
             V((2, 2 * hh, rows, 1), f32),
             V((2, 2 * hh, rows, dv), f32),
@@ -648,7 +710,7 @@
             V((GROUP, own, D), bf16),
             V((GROUP, own, D), bf16),
             V((2, own, D), bf16),
-            dma((4,)),
+            dma((5,)),
             dma((3,)),
             dma((2, 3)),
             dma((S,)),
@@ -656,8 +718,9 @@
             dma((2, Z // 2)),
             dma((2, S)),
             dma((2,)),
-            dma((2,)),
-            dma((2,)),
+            dma((2, 2)),
+            dma((2, 2)),
+            dma((2, 2)),
             dma((2, Z)),
             dma((T,)),
             dma((T,)),
@@ -667,18 +730,18 @@
             dma((GROUP, 3)),
             dma((GROUP,)),
             dma((GROUP,)),
-            dma((GROUP, 2)),
-            dma((GROUP, 2)),
-            dma((GROUP,)),
-            dma((GROUP,)),
-            dma((GROUP,)),
-            dma((2,)),
+            dma((GROUP, 2, SPLIT)),
+            dma((GROUP, 2, SPLIT)),
+            dma((GROUP, SPLIT)),
+            dma((GROUP, SPLIT)),
+            dma((GROUP, SPLIT)),
+            dma((2, SPLIT)),
         ],
         compiler_params=pltpu.CompilerParams(
             collective_id=0, has_side_effects=True, vmem_limit_bytes=64000000
         ),
     )(
-        q, kv, residual, w_out, w_gate, w_up, w_down, lambda_head,
+        queries, key_rows, values, residual, w_out, w_gate, w_up, w_down, lambda_head,
         sub_gain.reshape(1, -1), norm_gain.reshape(1, -1), conv_gate, conv_up,
     )
 

time: 144 us -> 126 us (0.88); the launches traced: 143 us -> 124 us
  Pallas kernels: 137 us -> 122 us
  local copies, waits for them, and re-layouts: 5.65 us -> 1.67 us
    pallas_call x1, Pallas kernels: 137 us -> 122 us  [local(): pl.pallas_call(functools.partial(kernel, S, T, heads, dh, dv), out_shape=...]
    reshape x4 -> x0, local copies, waits for them, and re-layouts: 3 us -> none  [the longest x2 1.85 us: local(): q = queries.reshape(rows, 2, hh * maps * dh).swapaxes(0, 1)]
where the time goes in v2:
time: 126 us; the launch traced here: 124 us
  Pallas kernels  122 us (97%)
  local copies, waits for them, and re-layouts  1.67 us (1%)
    pallas_call x1, Pallas kernels, local(): pl.pallas_call(functools.partial(kernel, S, T, heads, dh, dv), out_shape=...  122 us

profile of v2, /device:TPU:29, one launch (start us, length us, event | category | flops | bytes accessed | tf_op | source)
XLA Modules:
  0.0 123.8 jit_solution(5048047853882591244)
XLA Ops:
  0.0 122.1 %shard_map.127 = bf16[64,2048]{1,0:T(8,128)(2,1)} custom-call(bf16[256,2,2,128]{3,2,1,0:T(2,128)(2,1)} %q_hbm.1, bf16[256,2,2,128]{3,2,1,0:T(2,128)(2,1)} %k_hbm.1, bf16[256,2,256]{2,1,0:T(2,128)(2,1)} %v_hbm.1, bf16[256,2048]{1,0:T(8,128)(2,1)} %res_hbm.1, bf16[512,2048]{1,0:T(8,128)(2,1)} %wout_hbm.1, bf16[256,1408]{1,0:T(8,128)(2,1)} %wg_hbm.1, ...), custom_call_target="tpu_custom_call" | custom-call | tf_op jit(solution)/shard_map/pallas_call | solution.py:674
  122.1 1.7 %copy.15 = bf16[64,2048]{1,0:T(8,128)(2,1)} copy(bf16[64,2048]{1,0:T(8,128)(2,1)} %shard_map.127) | data formatting | bytes 524288

commit v3 on v2

--- a/solution.py
+++ b/solution.py
@@ -19,7 +19,7 @@
 HUBS = (1, 2)
 LANES = 128
 SPLIT = 2
-STAGED = {3: ((1, 0), (0, 0), (0, 1))}
+STAGED = {3: ((0, 0), (1, 0), (0, 1))}
 
 
 def scope(name):
@@ -39,11 +39,11 @@
     out_ref,
     q_raw, k_raw, v_raw, q_out, kv_out, q, kv, res, wout, wg, wu, wd, stage,
     m_s, l_s, acc_s, n_own, n_in, part, part_in, mid, hn,
-    g_s, u_s, halo_out, halo_in, hid, low, low_in, half, half_in, done, ret,
+    g_s, u_s, halo_out, halo_in, hid, low, low_in, half, half_in, done, ret, home_out, home_in,
     local_sem, own_sem, pair_sem, kv_send, kv_recv,
     w_send, w_recv, cross_send, lend_send, stage_recv, stage_send, relay_send,
     tp_send, tp_recv, hn_send, hn_recv, ag_send, ag_recv,
-    halo_send, halo_recv, core_send, core_recv, far_send, far_recv, ret_send, ret_recv,
+    halo_send, halo_recv, core_send, core_recv, far_send, far_recv, ret_send, ret_recv, home_send, home_recv, go_sem,
 ):
     Z = S // 2
     sp = lax.axis_index("sp")
@@ -213,18 +213,17 @@
         direct(i, 0).start()
         direct(i, 1).start()
 
+    def second(h):
+        return (zi == 3) & (h == z - 2)
+
     for i in reversed(range(len(targets))):
-        pl.when(z > targets[i][0])(functools.partial(direct_send, i))
-
-    def early(h):
-        return (zi == 1) & (h == z + 1)
-
-    for i in range(len(targets)):
-        pl.when(early(targets[i][0]))(lambda: direct(i, 0).start())
+        h = targets[i][0]
+        pl.when((z > h) & jnp.logical_not(second(h)))(functools.partial(direct_send, i))
 
     def cross_start(k):
         cross(k, 0).start()
-        cross(k, 1).start()
+        if k == 1:
+            cross(k, 1).start()
 
     as_hub(cross_start)
     each_staged(lambda k, w: lend(k, w).start())
@@ -308,20 +307,23 @@
 
             @pl.when((r == 1) & (zi == HUBS[1]))
             def _():
-                relay_from(z - 1, 0)
                 relay_from(z + 1, 1)
 
             @pl.when((r == 2) & (zi == 3))
             def _():
+                forward(0, 0)
+
+            @pl.when((r == 3) & (zi == 3))
+            def _():
                 forward(1, 0)
-                forward(0, 0)
-
-            pl.when((r == 3) & (zi == 3))(lambda: forward(0, 1))
+                forward(0, 1)
+
+            for i in range(len(targets)):
+                pl.when((r == 1) & second(targets[i][0]))(functools.partial(direct_send, i))
 
     for i in range(len(targets)):
         h = targets[i][0]
-        pl.when((z < h) & jnp.logical_not(early(h) | late(h)))(lambda: direct(i, 0).start())
-        pl.when((z < h) & jnp.logical_not(late(h)))(lambda: direct(i, 1).start())
+        pl.when((z < h) & jnp.logical_not(late(h)))(functools.partial(direct_send, i))
 
     with scope("nnorm"):
         for yy in range(2):
@@ -335,7 +337,11 @@
     n_swap = pair(n_own.at[other], n_in, 2)
     n_swap.start()
     with scope("relay1"):
-        pl.when(zi == HUBS[0])(lambda: relay_from(z + 1, 0))
+        @pl.when(zi == HUBS[0])
+        def _():
+            relay_from(z + 1, 0)
+            cross(0, 1).start()
+
     with scope("nswapw"):
         loads[3].wait()
         n_swap.wait_recv()
@@ -361,7 +367,7 @@
         c.start()
     twin = jnp.where(zi == HUBS[0], z + 1, z - 1)
     with scope("relayt"):
-        pl.when(hub)(lambda: relay_from(twin, 1))
+        pl.when(zi == HUBS[1])(lambda: relay_from(twin, 0))
     with scope("rs1"):
         loads[4].wait()
         total = res[...].astype(f32) + part[tp].astype(f32)
@@ -384,9 +390,14 @@
         )
 
     pl.when(zi != HUBS[0])(lambda: deliver(0).start())
-    pl.when(zi != HUBS[1])(lambda: deliver(1).start())
-    for i in range(len(targets)):
-        pl.when((z < targets[i][0]) & late(targets[i][0]))(functools.partial(direct_send, i))
+    pl.when((zi == 0) | (zi == 3))(lambda: deliver(1).start())
+
+    @pl.when(zi == 0)
+    def _():
+        pl.semaphore_wait(go_sem, 1)
+        for i in range(len(targets)):
+            pl.when(late(targets[i][0]))(functools.partial(direct_send, i))
+
 
     def spread(p, hop):
         src = (tp, tp, far_mate)[hop]
@@ -413,6 +424,8 @@
     with scope("relay2"):
         @pl.when(hub)
         def _():
+            gather1(0)
+            relay_from(twin, 1)
             for w in range(2):
                 @pl.loop(0, Z)
                 def _(i):
@@ -458,6 +471,19 @@
         at = slice(h * side, (h + 1) * side)
         half[p, :, at] = (low[p, far_mate, :, at].astype(f32) + low_in[p, 1, :, at].astype(f32)).astype(bf16)
         far_copy(p, h).start()
+
+    def home_copy(k, i, h):
+        return remote(
+            home_out.at[i, :, span(h)], home_in.at[k, i, :, span(h)],
+            home_send.at[i, h], home_recv.at[k, i, h], (base * 2 + y, tp),
+        )
+
+    def send_home(h):
+        at = slice(h * side, (h + 1) * side)
+        for i, t in ((1, far_mate), (0, tp)):
+            core_copy(0, i, h).wait_recv()
+            home_out[i, :, at] = (low[0, t, :, at].astype(f32) + low_in[0, i, :, at].astype(f32)).astype(bf16)
+            as_hub(lambda k: home_copy(k, i, h).start())
 
     def reduce2(p, h):
         core_copy(p, 0, h).wait_recv()
@@ -487,11 +513,36 @@
         halo_out[p, 1] = u_s[rows:, :].astype(bf16)
         pl.when(halo_sends(p))(lambda: halo_copy(p).start())
 
+        lo = jnp.where(zi == HUBS[0], pieces[0][0], pieces[1][0])
+
+        def conv(start, count):
+            for c in range(0, cap, LANES):
+                at = slice(c, c + LANES)
+                tap = pl.ds(pl.multiple_of(jnp.minimum(lo + c, units - LANES), LANES), LANES)
+
+                def mix(x, taps):
+                    at0 = HALO + start
+                    out = taps[0:1, tap] * x[at0 - 2 : at0 - 2 + count, at]
+                    out = out + taps[1:2, tap] * x[at0 - 1 : at0 - 1 + count, at]
+                    return out + taps[2:3, tap] * x[at0 : at0 + count, at]
+
+                gm, um = mix(g_s, cg_ref), mix(u_s, cu_ref)
+                hid[start : start + count, at] = (gm / (1.0 + jnp.exp(-gm)) * um).astype(bf16)
+
         @pl.when(p > 0)
         def _():
-            for h in range(SPLIT):
-                reduce1(p - 1, h)
-
+            @pl.when(p == 1)
+            def _():
+                for h in range(SPLIT):
+                    send_home(h)
+
+            @pl.when(p > 1)
+            def _():
+                reduce1(p - 1, 0)
+                pl.when(p < GROUP - 1)(lambda: reduce1(p - 1, 1))
+
+        conv(HALO, rows - HALO)
+        pl.when(p == GROUP - 2)(lambda: gather2(GROUP - 1))
         first = (y == 0) & (p == 0) & (base == 0)
 
         @pl.when(first)
@@ -501,22 +552,12 @@
 
         @pl.when(jnp.logical_not(first))
         def _():
-            remote(halo_out.at[p], halo_in.at[p], halo_send.at[p], halo_recv.at[p], (mate, tp)).wait_recv()
+            with scope("halo"):
+                remote(halo_out.at[p], halo_in.at[p], halo_send.at[p], halo_recv.at[p], (mate, tp)).wait_recv()
             g_s[:HALO, :] = halo_in[p, 0].astype(f32)
             u_s[:HALO, :] = halo_in[p, 1].astype(f32)
 
-        lo = jnp.where(zi == HUBS[0], pieces[0][0], pieces[1][0])
-        for c in range(0, cap, LANES):
-            at = slice(c, c + LANES)
-            tap = pl.ds(pl.multiple_of(jnp.minimum(lo + c, units - LANES), LANES), LANES)
-
-            def mix(x, taps):
-                out = taps[0:1, tap] * x[HALO - 2 : HALO - 2 + rows, at]
-                out = out + taps[1:2, tap] * x[HALO - 1 : HALO - 1 + rows, at]
-                return out + taps[2:3, tap] * x[HALO:, at]
-
-            gm, um = mix(g_s, cg_ref), mix(u_s, cu_ref)
-            hid[:, at] = (gm / (1.0 + jnp.exp(-gm)) * um).astype(bf16)
+        conv(0, HALO)
         for c in range(0, D, width):
             at = slice(c, c + width)
             low[p, :, :, at] = (
@@ -544,35 +585,35 @@
 
         down_piece(k).wait()
 
+    with scope("go"):
+        @pl.when(zi == HUBS[0])
+        def _():
+            for i in range(len(targets)):
+                @pl.when(targets[i][0] == z + 1)
+                def _():
+                    direct(i, 0).wait_send()
+                    direct(i, 1).wait_send()
+
+            pl.semaphore_signal(go_sem, inc=1, device_id=(sp - 2, tp), device_id_type=MESH)
+            deliver(1).start()
+
     @pl.when(hub)
     def _():
         with scope("ga"):
-            pl.when(zi != HUBS[0])(lambda: gather1(HUBS[0]))
-            gather1(0)
             gather2(zi)
-            pl.when(zi != HUBS[0])(lambda: gather2(HUBS[0]))
-            pl.when(zi != HUBS[1])(lambda: gather1(HUBS[1]))
             gather2(0)
+            pl.when(zi == HUBS[0])(lambda: gather1(HUBS[1]))
+            pl.when(zi == HUBS[1])(lambda: gather1(HUBS[0]))
 
         with scope("wwait"):
             as_hub(wait_pieces)
 
         @pl.loop(0, GROUP)
         def _(p):
-            @pl.when(p == 0)
-            def _():
-                with scope("gather2"):
-                    gather1(GROUP - 1)
-
-            @pl.when(p == 1)
-            def _():
-                with scope("gather3"):
-                    pl.when(zi != HUBS[1])(lambda: gather2(HUBS[1]))
-
-            @pl.when(p == 2)
-            def _():
-                with scope("gather4"):
-                    gather2(GROUP - 1)
+            other_hub = jnp.where(zi == HUBS[0], HUBS[1], HUBS[0])
+            with scope("gat"):
+                pl.when(p == 0)(lambda: gather1(GROUP - 1))
+                pl.when(p == other_hub)(lambda: gather2(other_hub))
 
             with scope("agw"):
                 spread(p, 1).wait_recv()
@@ -581,25 +622,42 @@
                 feed(p)
 
         with scope("redlast"):
+            for p, h in ((3, 0), (3, 1), (2, 1)):
+                with scope("r1"):
+                    reduce1(p, h)
+            for p, h in ((1, 0), (1, 1), (2, 0), (3, 0), (3, 1), (2, 1)):
+                with scope(f"r2{p}{h}"):
+                    reduce2(p, h)
+
+    with scope("final"):
+        @pl.when(zi == 0)
+        def _():
             for h in range(SPLIT):
-                with scope("r13"):
-                    reduce1(GROUP - 1, h)
-            for p in range(GROUP):
-                for h in range(SPLIT):
-                    with scope(f"r2{p}{h}"):
-                        reduce2(p, h)
-
-    with scope("final"):
-        for h in range(SPLIT):
-            at = slice(h * side, (h + 1) * side)
-            total = mid[:, at]
-            for k in range(2):
-                got = remote(
-                    done.at[0, :, span(h)], ret.at[k, :, span(h)], ret_send.at[0, h], ret_recv.at[k, h], (sp, tp)
-                )
-                pl.when(zi != HUBS[k])(got.wait_recv)
-                total = total + ret[k, :, at].astype(f32)
-            out_ref[:, at] = total.astype(bf16)
+                at = slice(h * side, (h + 1) * side)
+                for k in range(2):
+                    home_copy(k, 1, h).wait_recv()
+                half[0, :, at] = (home_in[0, 1, :, at].astype(f32) + home_in[1, 1, :, at].astype(f32)).astype(bf16)
+                far_copy(0, h).start()
+            for h in range(SPLIT):
+                at = slice(h * side, (h + 1) * side)
+                for k in range(2):
+                    home_copy(k, 0, h).wait_recv()
+                total = mid[:, at] + home_in[0, 0, :, at].astype(f32) + home_in[1, 0, :, at].astype(f32)
+                far_copy(0, h).wait_recv()
+                out_ref[:, at] = (total + half_in[0, :, at].astype(f32)).astype(bf16)
+
+        @pl.when(zi != 0)
+        def _():
+            for h in range(SPLIT):
+                at = slice(h * side, (h + 1) * side)
+                total = mid[:, at]
+                for k in range(2):
+                    got = remote(
+                        done.at[0, :, span(h)], ret.at[k, :, span(h)], ret_send.at[0, h], ret_recv.at[k, h], (sp, tp)
+                    )
+                    pl.when(zi != HUBS[k])(got.wait_recv)
+                    total = total + ret[k, :, at].astype(f32)
+                out_ref[:, at] = total.astype(bf16)
 
     with scope("drain"):
         @pl.loop(0, Z)
@@ -616,7 +674,7 @@
             as_hub(go)
 
         for i in range(len(targets)):
-            @pl.when(z != targets[i][0])
+            @pl.when((z != targets[i][0]) & ((zi != HUBS[0]) | (targets[i][0] != z + 1)))
             def _():
                 direct(i, 0).wait_send()
                 direct(i, 1).wait_send()
@@ -637,8 +695,17 @@
         for k in range(2):
             pl.when(zi != HUBS[k])(lambda: deliver(k).wait_send())
 
+        @pl.when(zi == 0)
+        def _():
+            for h in range(SPLIT):
+                far_copy(0, h).wait_send()
+
         @pl.when(hub)
         def _():
+            for h in range(SPLIT):
+                for i in range(2):
+                    home_copy(0, i, h).wait_send()
+
             @pl.loop(0, GROUP)
             def _(p):
                 for hop in range(3):
@@ -647,8 +714,8 @@
                 for h in range(SPLIT):
                     core_copy(p, 0, h).wait_send()
                     core_copy(p, 1, h).wait_send()
-                    far_copy(p, h).wait_send()
-                    pl.when(p != zi)(give_back(p, 0, h).wait_send)
+                    pl.when(p > 0)(far_copy(p, h).wait_send)
+                    pl.when((p > 0) & (p != zi))(give_back(p, 0, h).wait_send)
 
 
 def local(
@@ -710,6 +777,8 @@
             V((GROUP, own, D), bf16),
             V((GROUP, own, D), bf16),
             V((2, own, D), bf16),
+            V((2, own, D), bf16),
+            V((2, 2, own, D), bf16),
             dma((5,)),
             dma((3,)),
             dma((2, 3)),
@@ -736,6 +805,9 @@
             dma((GROUP, SPLIT)),
             dma((GROUP, SPLIT)),
             dma((2, SPLIT)),
+            dma((2, SPLIT)),
+            dma((2, 2, SPLIT)),
+            pltpu.SemaphoreType.REGULAR,
         ],
         compiler_params=pltpu.CompilerParams(
             collective_id=0, has_side_effects=True, vmem_limit_bytes=64000000

time: 126 us -> 117 us (0.929); the launches traced: 124 us -> 117 us
  Pallas kernels: 122 us -> 116 us
    pallas_call x1, Pallas kernels: 122 us -> 116 us  [local(): pl.pallas_call(functools.partial(kernel, S, T, heads, dh, dv), out_shape=...]
where the time goes in v3:
time: 117 us
  Pallas kernels  116 us (99%)
  local copies, waits for them, and re-layouts  1.67 us (1%)
    pallas_call x1, Pallas kernels, local(): pl.pallas_call(functools.partial(kernel, S, T, heads, dh, dv), out_shape=...  116 us

profile of v3, /device:TPU:29, one launch (start us, length us, event | category | flops | bytes accessed | tf_op | source)
XLA Modules:
  0.0 117.2 jit_solution(10747951715376162687)
XLA Ops:
  0.0 115.5 %shard_map.127 = bf16[64,2048]{1,0:T(8,128)(2,1)} custom-call(bf16[256,2,2,128]{3,2,1,0:T(2,128)(2,1)} %q_hbm.1, bf16[256,2,2,128]{3,2,1,0:T(2,128)(2,1)} %k_hbm.1, bf16[256,2,256]{2,1,0:T(2,128)(2,1)} %v_hbm.1, bf16[256,2048]{1,0:T(8,128)(2,1)} %res_hbm.1, bf16[512,2048]{1,0:T(8,128)(2,1)} %wout_hbm.1, bf16[256,1408]{1,0:T(8,128)(2,1)} %wg_hbm.1, ...), custom_call_target="tpu_custom_call" | custom-call | tf_op jit(solution)/shard_map/pallas_call | solution.py:741
  115.5 1.7 %copy.15 = bf16[64,2048]{1,0:T(8,128)(2,1)} copy(bf16[64,2048]{1,0:T(8,128)(2,1)} %shard_map.127) | data formatting | bytes 524288

commit v4 on v3

--- a/solution.py
+++ b/solution.py
@@ -485,6 +485,12 @@
             home_out[i, :, at] = (low[0, t, :, at].astype(f32) + low_in[0, i, :, at].astype(f32)).astype(bf16)
             as_hub(lambda k: home_copy(k, i, h).start())
 
+    def lift(h):
+        return remote(
+            done.at[GROUP - 1, :, span(h)], home_in.at[0, 0, :, span(h)],
+            ret_send.at[GROUP - 1, h], home_recv.at[0, 0, h], ((base + HUBS[1]) * 2 + y, tp),
+        )
+
     def reduce2(p, h):
         core_copy(p, 0, h).wait_recv()
         far_copy(p, h).wait_recv()
@@ -492,6 +498,16 @@
         t = low[p, tp, :, at].astype(f32) + low_in[p, 0, :, at].astype(f32) + half_in[p, :, at].astype(f32)
 
         def hand(k):
+            if p == GROUP - 1 and k == 0:
+                done[p, :, at] = t.astype(bf16)
+                lift(h).start()
+                return
+            if p == GROUP - 1:
+                lift(h).wait_recv()
+                done[p, :, at] = (t + home_in[0, 0, :, at].astype(f32)).astype(bf16)
+                give_back(p, k, h).start()
+                return
+
             @pl.when(p == zi)
             def _():
                 ret[k, :, at] = t.astype(bf16)
@@ -536,10 +552,10 @@
                 for h in range(SPLIT):
                     send_home(h)
 
-            @pl.when(p > 1)
-            def _():
-                reduce1(p - 1, 0)
-                pl.when(p < GROUP - 1)(lambda: reduce1(p - 1, 1))
+            @pl.when(p == 2)
+            def _():
+                for h in range(SPLIT):
+                    reduce1(1, h)
 
         conv(HALO, rows - HALO)
         pl.when(p == GROUP - 2)(lambda: gather2(GROUP - 1))
@@ -591,8 +607,10 @@
             for i in range(len(targets)):
                 @pl.when(targets[i][0] == z + 1)
                 def _():
-                    direct(i, 0).wait_send()
-                    direct(i, 1).wait_send()
+                    with scope("gog"):
+                        direct(i, 0).wait_send()
+                    with scope("gou"):
+                        direct(i, 1).wait_send()
 
             pl.semaphore_signal(go_sem, inc=1, device_id=(sp - 2, tp), device_id_type=MESH)
             deliver(1).start()
@@ -612,8 +630,9 @@
         def _(p):
             other_hub = jnp.where(zi == HUBS[0], HUBS[1], HUBS[0])
             with scope("gat"):
-                pl.when(p == 0)(lambda: gather1(GROUP - 1))
+                pl.when(p == jnp.where(zi == HUBS[0], 1, 0))(lambda: gather1(GROUP - 1))
                 pl.when(p == other_hub)(lambda: gather2(other_hub))
+                pl.when(p == GROUP - 1)(lambda: reduce1(GROUP - 2, 0))
 
             with scope("agw"):
                 spread(p, 1).wait_recv()
@@ -646,7 +665,16 @@
                 far_copy(0, h).wait_recv()
                 out_ref[:, at] = (total + half_in[0, :, at].astype(f32)).astype(bf16)
 
-        @pl.when(zi != 0)
+        @pl.when(zi == GROUP - 1)
+        def _():
+            for h in range(SPLIT):
+                at = slice(h * side, (h + 1) * side)
+                remote(
+                    done.at[0, :, span(h)], ret.at[1, :, span(h)], ret_send.at[0, h], ret_recv.at[1, h], (sp, tp)
+                ).wait_recv()
+                out_ref[:, at] = (mid[:, at] + ret[1, :, at].astype(f32)).astype(bf16)
+
+        @pl.when(hub)
         def _():
             for h in range(SPLIT):
                 at = slice(h * side, (h + 1) * side)

time: 117 us -> 113 us (0.966)
  Pallas kernels: 116 us -> 111 us
    pallas_call x1, Pallas kernels: 116 us -> 111 us  [local(): pl.pallas_call(functools.partial(kernel, S, T, heads, dh, dv), out_shape=...]
where the time goes in v4:
time: 113 us
  Pallas kernels  111 us (98%)
  local copies, waits for them, and re-layouts  1.67 us (1%)
    pallas_call x1, Pallas kernels, local(): pl.pallas_call(functools.partial(kernel, S, T, heads, dh, dv), out_shape=...  111 us

profile of v4, /device:TPU:29, one launch (start us, length us, event | category | flops | bytes accessed | tf_op | source)
XLA Modules:
  0.0 112.7 jit_solution(12459806250035136867)
XLA Ops:
  0.0 111.0 %shard_map.127 = bf16[64,2048]{1,0:T(8,128)(2,1)} custom-call(bf16[256,2,2,128]{3,2,1,0:T(2,128)(2,1)} %q_hbm.1, bf16[256,2,2,128]{3,2,1,0:T(2,128)(2,1)} %k_hbm.1, bf16[256,2,256]{2,1,0:T(2,128)(2,1)} %v_hbm.1, bf16[256,2048]{1,0:T(8,128)(2,1)} %res_hbm.1, bf16[512,2048]{1,0:T(8,128)(2,1)} %wout_hbm.1, bf16[256,1408]{1,0:T(8,128)(2,1)} %wg_hbm.1, ...), custom_call_target="tpu_custom_call" | custom-call | tf_op jit(solution)/shard_map/pallas_call | solution.py:769
  111.0 1.7 %copy.15 = bf16[64,2048]{1,0:T(8,128)(2,1)} copy(bf16[64,2048]{1,0:T(8,128)(2,1)} %shard_map.127) | data formatting | bytes 524288

commit v5 on v4

--- a/solution.py
+++ b/solution.py
@@ -43,7 +43,7 @@
     local_sem, own_sem, pair_sem, kv_send, kv_recv,
     w_send, w_recv, cross_send, lend_send, stage_recv, stage_send, relay_send,
     tp_send, tp_recv, hn_send, hn_recv, ag_send, ag_recv,
-    halo_send, halo_recv, core_send, core_recv, far_send, far_recv, ret_send, ret_recv, home_send, home_recv, go_sem,
+    halo_send, halo_recv, core_send, core_recv, far_send, far_recv, ret_send, ret_recv, home_send, home_recv, go_sem, mate_sem,
 ):
     Z = S // 2
     sp = lax.axis_index("sp")
@@ -82,8 +82,13 @@
     def cols(k):
         return pl.ds(pieces[k][0], pieces[k][1])
 
-    def block(b, k):
-        return (pl.ds(pl.multiple_of(b * feat, feat), feat), pl.ds(0, pieces[k][1]))
+    cut = feat // 2
+
+    def part_rows(w):
+        return pl.ds((w % 2) * cut, cut)
+
+    def block(b, k, w):
+        return (pl.ds(pl.multiple_of(b * feat + (w % 2) * cut, cut), cut), pl.ds(0, pieces[k][1]))
 
     sources, stores = (wg_hbm, wu_hbm), (wg, wu)
     targets = [(g * GROUP + HUBS[k], k) for g in range(Z // GROUP) for k in range(2)]
@@ -91,50 +96,51 @@
     def direct(i, w):
         h, k = targets[i]
         return remote(
-            sources[w].at[:, cols(k)], stores[w].at[block(sp, k)],
+            sources[w // 2].at[part_rows(w), cols(k)], stores[w // 2].at[block(sp, k, w)],
             w_send.at[w, i], w_recv.at[w, sp], (h * 2 + y, tp),
         )
 
     def cross(k, w):
         return remote(
-            sources[w].at[:, cols(k)], stores[w].at[block(sp, k)],
+            sources[w // 2].at[part_rows(w), cols(k)], stores[w // 2].at[block(sp, k, w)],
             cross_send.at[w], w_recv.at[w, sp], (mate, tp),
         )
 
     def lend(k, w):
         return remote(
-            sources[w].at[:, cols(k)], stage.at[k, w, :, pl.ds(0, pieces[k][1])],
+            sources[w // 2].at[part_rows(w), cols(k)], stage.at[k, w // 2, part_rows(w), pl.ds(0, pieces[k][1])],
             lend_send.at[k, w], stage_recv.at[k, w], (mate, tp),
         )
 
     def pass_on(k, w):
         h = base + HUBS[k]
         return remote(
-            stage.at[k, w, :, pl.ds(0, pieces[k][1])], stores[w].at[block(mate, k)],
+            stage.at[k, w // 2, part_rows(w), pl.ds(0, pieces[k][1])], stores[w // 2].at[block(mate, k, w)],
             stage_send.at[k, w], w_recv.at[w, mate], (h * 2 + y, tp),
         )
 
     def staged(zz, k, w):
         hit = zz < 0
         for zo, which in STAGED.items():
-            if (k, w) in which:
+            if (k, w // 2) in which:
                 hit = hit | (zz == base + zo)
         return hit
 
     def each_staged(fn):
         for zo, which in STAGED.items():
             for k, w in which:
-                pl.when(zi == zo)(functools.partial(fn, k, w))
+                pl.when(zi == zo)(functools.partial(fn, k, 2 * w))
+                pl.when(zi == zo)(functools.partial(fn, k, 2 * w + 1))
 
     def relay(zz, k, w):
         b = zz * 2 + y
         return remote(
-            stores[w].at[block(b, k)], stores[w].at[block(b, k)],
+            stores[w // 2].at[block(b, k, w)], stores[w // 2].at[block(b, k, w)],
             relay_send.at[w, zz], w_recv.at[w, b], (mate, tp),
         )
 
     def own_piece(k, w):
-        return pltpu.make_async_copy(sources[w].at[:, cols(k)], stores[w].at[block(sp, k)], own_sem.at[w])
+        return pltpu.make_async_copy(sources[w].at[:, cols(k)], stores[w].at[pl.ds(pl.multiple_of(sp * feat, feat), feat), pl.ds(0, pieces[k][1])], own_sem.at[w])
 
     def down_piece(k):
         return pltpu.make_async_copy(
@@ -210,8 +216,8 @@
     send_up(sp)
 
     def direct_send(i):
-        direct(i, 0).start()
-        direct(i, 1).start()
+        for w in range(4):
+            direct(i, w).start()
 
     def second(h):
         return (zi == 3) & (h == z - 2)
@@ -221,16 +227,16 @@
         pl.when((z > h) & jnp.logical_not(second(h)))(functools.partial(direct_send, i))
 
     def cross_start(k):
-        cross(k, 0).start()
-        if k == 1:
-            cross(k, 1).start()
+        for w in range(4 if k == 1 else 2):
+            cross(k, w).start()
 
     as_hub(cross_start)
     each_staged(lambda k, w: lend(k, w).start())
 
     def forward(k, w):
-        lend(k, w).wait_recv()
-        pass_on(k, w).start()
+        for part in (2 * w, 2 * w + 1):
+            lend(k, part).wait_recv()
+            pass_on(k, part).start()
 
     m_s[...] = jnp.full(m_s.shape, -1e30, f32)
     l_s[...] = jnp.zeros(l_s.shape, f32)
@@ -273,13 +279,14 @@
     def late(h):
         return (zi == 0) & (h > z + 1)
 
-    def relay_from(zz, w):
+    def relay_from(zz, which):
         def go(k):
-            @pl.when((zz != z) & jnp.logical_not(staged(zz, k, w)))
-            def _():
-                with scope("rly"):
-                    relay(zz, k, w).wait_recv()
-                relay(zz, k, w).start()
+            @pl.when((zz != z) & jnp.logical_not(staged(zz, k, 2 * which)))
+            def _():
+                for w in (2 * which, 2 * which + 1):
+                    with scope("rly"):
+                        relay(zz, k, w).wait_recv()
+                    relay(zz, k, w).start()
 
         as_hub(go)
 
@@ -340,7 +347,8 @@
         @pl.when(zi == HUBS[0])
         def _():
             relay_from(z + 1, 0)
-            cross(0, 1).start()
+            cross(0, 2).start()
+            cross(0, 3).start()
 
     with scope("nswapw"):
         loads[3].wait()
@@ -584,13 +592,13 @@
                 core_copy(p, 0, c // side).start()
 
     def wait_pieces(k):
-        for w in range(2):
-            own_piece(k, w).wait()
+        own_piece(k, 0).wait()
+        own_piece(k, 1).wait()
+        for w in range(4):
 
             def arrived(b):
-              with scope("arrw"):
                 remote(
-                    stores[w].at[block(b, k)], stores[w].at[block(b, k)],
+                    stores[w // 2].at[block(b, k, w)], stores[w // 2].at[block(b, k, w)],
                     cross_send.at[w], w_recv.at[w, b], (mate, tp),
                 ).wait_recv()
 
@@ -607,11 +615,11 @@
             for i in range(len(targets)):
                 @pl.when(targets[i][0] == z + 1)
                 def _():
-                    with scope("gog"):
-                        direct(i, 0).wait_send()
-                    with scope("gou"):
-                        direct(i, 1).wait_send()
-
+                    for w in range(4):
+                        direct(i, w).wait_send()
+
+            pl.semaphore_signal(mate_sem, inc=1, device_id=(sp, core_mate), device_id_type=MESH)
+            pl.semaphore_wait(mate_sem, 1)
             pl.semaphore_signal(go_sem, inc=1, device_id=(sp - 2, tp), device_id_type=MESH)
             deliver(1).start()
 
@@ -630,7 +638,7 @@
         def _(p):
             other_hub = jnp.where(zi == HUBS[0], HUBS[1], HUBS[0])
             with scope("gat"):
-                pl.when(p == jnp.where(zi == HUBS[0], 1, 0))(lambda: gather1(GROUP - 1))
+                pl.when(p == 1)(lambda: gather1(GROUP - 1))
                 pl.when(p == other_hub)(lambda: gather2(other_hub))
                 pl.when(p == GROUP - 1)(lambda: reduce1(GROUP - 2, 0))
 
@@ -696,7 +704,7 @@
                 climb(2 * zz + 1).wait_send()
 
             def go(k):
-                for w in range(2):
+                for w in range(4):
                     pl.when((zz != z) & jnp.logical_not(staged(zz, k, w)))(relay(zz, k, w).wait_send)
 
             as_hub(go)
@@ -704,12 +712,12 @@
         for i in range(len(targets)):
             @pl.when((z != targets[i][0]) & ((zi != HUBS[0]) | (targets[i][0] != z + 1)))
             def _():
-                direct(i, 0).wait_send()
-                direct(i, 1).wait_send()
+                for w in range(4):
+                    direct(i, w).wait_send()
 
         def cross_end(k):
-            cross(k, 0).wait_send()
-            cross(k, 1).wait_send()
+            for w in range(4):
+                cross(k, w).wait_send()
 
         as_hub(cross_end)
 
@@ -812,13 +820,13 @@
             dma((2, 3)),
             dma((S,)),
             dma((S,)),
-            dma((2, Z // 2)),
-            dma((2, S)),
-            dma((2,)),
-            dma((2, 2)),
-            dma((2, 2)),
-            dma((2, 2)),
-            dma((2, Z)),
+            dma((4, Z // 2)),
+            dma((4, S)),
+            dma((4,)),
+            dma((2, 4)),
+            dma((2, 4)),
+            dma((2, 4)),
+            dma((4, Z)),
             dma((T,)),
             dma((T,)),
             dma((2,)),
@@ -835,6 +843,7 @@
             dma((2, SPLIT)),
             dma((2, SPLIT)),
             dma((2, 2, SPLIT)),
+            pltpu.SemaphoreType.REGULAR,
             pltpu.SemaphoreType.REGULAR,
         ],
         compiler_params=pltpu.CompilerParams(

time: 113 us -> 113 us (level); the launches traced: 113 us -> 111 us
  Pallas kernels: 111 us -> 109 us
    pallas_call x1, Pallas kernels: 111 us -> 109 us  [local(): pl.pallas_call(functools.partial(kernel, S, T, heads, dh, dv), out_shape=...]
where the time goes in v5:
time: 113 us; the launch traced here: 111 us
  Pallas kernels  109 us (96%)
  local copies, waits for them, and re-layouts  1.67 us (1%)
    pallas_call x1, Pallas kernels, local(): pl.pallas_call(functools.partial(kernel, S, T, heads, dh, dv), out_shape=...  109 us

profile of v5, /device:TPU:29, one launch (start us, length us, event | category | flops | bytes accessed | tf_op | source)
XLA Modules:
  0.0 110.8 jit_solution(6390673101469657669)
XLA Ops:
  0.0 109.1 %shard_map.127 = bf16[64,2048]{1,0:T(8,128)(2,1)} custom-call(bf16[256,2,2,128]{3,2,1,0:T(2,128)(2,1)} %q_hbm.1, bf16[256,2,2,128]{3,2,1,0:T(2,128)(2,1)} %k_hbm.1, bf16[256,2,256]{2,1,0:T(2,128)(2,1)} %v_hbm.1, bf16[256,2048]{1,0:T(8,128)(2,1)} %res_hbm.1, bf16[512,2048]{1,0:T(8,128)(2,1)} %wout_hbm.1, bf16[256,1408]{1,0:T(8,128)(2,1)} %wg_hbm.1, ...), custom_call_target="tpu_custom_call" | custom-call | tf_op jit(solution)/shard_map/pallas_call | solution.py:777
  109.1 1.7 %copy.15 = bf16[64,2048]{1,0:T(8,128)(2,1)} copy(bf16[64,2048]{1,0:T(8,128)(2,1)} %shard_map.127) | data formatting | bytes 524288
